TPU v7x, 256 devices: a whole 4x4x8 slice. The times are simulated.
256 devices in a mesh: sp: 64 (over z, y, core), tp: 4 (over x).
Axes of the slice: x: 4, y: 4, z: 8, core: 2. Of those that a mesh axis runs over, the one named last changes fastest.
Arguments:
- glu_value: bfloat16 [32768, 2048], P('sp', 'tp'), may hold values from -640 to 640
- glu_gate: bfloat16 [32768, 2048], P('sp', 'tp'), may hold values from -9 to 9
- conv_kernel: float32 [31, 2048], P(None, 'tp'), may hold values from -1 to 1
- norm_gain: float32 [2048], P('tp'), may hold values from 0.1 to 1.9
- mix_weight: bfloat16 [2048, 2048], P('tp'), may hold values from -0.125 to 0.125
- residual: bfloat16 [32768, 2048], P(('sp', 'tp')), may hold values from -6 to 6
- resid_gain: float32 [2048], replicated, may hold values from 0.1 to 1.9
- expert_ids: int32 [32768, 2], P(('sp', 'tp')), may hold values from 0 to 63, all different within a row; in each aligned block of 128 rows (0 to 127, 128 to 255, ...) at most 8 rows name the same one
- route_weight: float32 [32768, 2], P(('sp', 'tp')), may hold values from 0.05 to 0.5
- w_gate: bfloat16 [64, 2048, 2048], P('sp', None, 'tp'), may hold values from -0.5 to 0.5
- w_up: bfloat16 [64, 2048, 2048], P('sp', None, 'tp'), may hold values from -0.5 to 0.5
- w_down: bfloat16 [64, 2048, 2048], P('sp', 'tp'), may hold values from -0.03125 to 0.03125
- out_gain: float32 [2048], replicated, may hold values from 0.1 to 1.9
Outputs:
- blended: bfloat16 [32768, 2048], P(('sp', 'tp'))
Inputs may be any that keep to these rules, and one draw needn't show every extreme that they name: `expert_ids`: in each aligned block of 128 rows (the rows of one device) no expert is named by more than 8 rows, a bound that some block reaches.
All inputs are finite; a program needn't handle non-finite values.
Results may differ from a plain program's by a relative error of at most 0.015.
Values may be sent and summed in bfloat16 or wider, within the bound.
A program may use at most 128 MiB of HBM per device.

v0:
```python
import jax
import jax.numpy as jnp
from jax import lax
from jax.sharding import PartitionSpec as P

DC = 2048


EPSILON = 1e-05
LIMIT = 7.0
SLOPE = 1.702


def shifted(block, axis, distance):
    devices = range(lax.axis_size(axis))
    route = [(i - distance, i) for i in devices if i - distance in devices]
    return lax.ppermute(block, axis, route)


def copy_for_each(array, axis):
    count = lax.axis_size(axis)
    return lax.all_to_all(
        jnp.broadcast_to(array[None], (count, *array.shape)), axis, 0, 0, tiled=True
    )


def of_everyone(array, axis):
    return copy_for_each(array, axis).sum(axis=0)


def together(arrays, axis):
    ends = [0]
    for a in arrays:
        ends.append(ends[-1] + a.size)
    running = of_everyone(jnp.concatenate([a.ravel() for a in arrays]), axis)
    return tuple((running[b:e].reshape(a.shape) for a, b, e in zip(arrays, ends, ends[1:])))


def cut_along(array, dim, count):
    before, after = (array.shape[:dim], array.shape[dim + 1 :])
    return jnp.moveaxis(array.reshape(*before, count, -1, *after), dim, 0)


def sum_at_owner(array, axis, dim):
    tiles = cut_along(array, dim, lax.axis_size(axis))
    arrived = lax.all_to_all(tiles, axis, split_axis=0, concat_axis=0, tiled=True)
    return arrived.astype(jnp.float32).sum(axis=0)


def in_order(tiles, dim):
    dims = list(tiles.shape[1:])
    dims[dim] *= tiles.shape[0]
    return jnp.moveaxis(tiles, 0, dim).reshape(dims)


def work_in_pieces(array, axis, dim, apply, out_dim):
    size, extent = (lax.axis_size(axis), array.shape[dim])
    count = 2 if extent % 2 == 0 else 1
    done, length = ([], extent // count)
    for k in range(count):
        section = lax.slice_in_dim(array, k * length, (k + 1) * length, axis=dim)
        starts = jnp.arange(size) * extent + k * length
        done.append(jax.vmap(apply)(lax.all_gather(section, axis), starts))
    return in_order(jnp.concatenate(done, axis=out_dim + 1), out_dim)


def normalize(values, gain_vector):
    centre = jnp.mean(values, axis=-1, keepdims=True)
    spread = jnp.mean(jnp.square(values - centre), axis=-1, keepdims=True)
    return (values - centre) * lax.rsqrt(spread + EPSILON) * gain_vector


def slot_layout(route_ids, experts, capacity):
    row_count, top_count = route_ids.shape
    flat_ids = route_ids.reshape(row_count * top_count)
    onehot = (flat_ids[:, None] == jnp.arange(experts, dtype=jnp.int32)[None, :]).astype(jnp.int32)
    before = jnp.cumsum(onehot, axis=0) - onehot
    slot_rank = jnp.sum(before * onehot, axis=1)
    position = flat_ids * capacity + slot_rank
    owners = jnp.arange(row_count * top_count, dtype=jnp.int32) // top_count
    slot_table = jnp.full((experts * capacity,), row_count, jnp.int32).at[position].set(owners)
    return (slot_table, position.reshape(row_count, top_count))


def expert_activity(tokens, gate_matrix, up_matrix):
    gate_pre = jnp.dot(tokens, gate_matrix, preferred_element_type=jnp.float32)
    up_pre = jnp.dot(tokens, up_matrix, preferred_element_type=jnp.float32)
    gated = jnp.minimum(gate_pre, LIMIT)
    upper = jnp.clip(up_pre, -LIMIT, LIMIT)
    return ((upper + 1.0) * gated * jax.nn.sigmoid(SLOPE * gated)).astype(jnp.bfloat16)


def shards(
    glu_value,
    glu_gate,
    conv_kernel,
    norm_gain,
    mix_weight,
    residual,
    resid_gain,
    expert_ids,
    route_weight,
    w_gate,
    w_up,
    w_down,
    out_gain,
):
    gated_in = (
        glu_value.astype(jnp.float32) * jax.nn.sigmoid(glu_gate.astype(jnp.float32))
    ).astype(jnp.bfloat16)
    reach_back = conv_kernel.shape[0] - 1
    length = gated_in.shape[0]
    before_rows = shifted(gated_in[length - reach_back :], "sp", 1)
    extended = jnp.concatenate([before_rows, gated_in], axis=0).astype(jnp.float32)
    convolved = jnp.zeros(gated_in.shape, jnp.float32)
    for offset in range(reach_back + 1):
        convolved = convolved + conv_kernel[offset] * extended[offset : offset + length]
    channel_sum, squares = together(
        (jnp.sum(convolved, axis=1), jnp.sum(convolved * convolved, axis=1)), "tp"
    )
    centre = channel_sum / DC
    spread = squares / DC - centre * centre
    normed = (convolved - centre[:, None]) * lax.rsqrt(spread[:, None] + EPSILON) * norm_gain
    mix_in = jax.nn.silu(normed).astype(jnp.bfloat16)
    tp_count = lax.axis_size("tp")
    own_count = length // tp_count
    section = mix_in
    mixed_rows = sum_at_owner(
        jnp.dot(section, mix_weight, preferred_element_type=jnp.float32).astype(jnp.bfloat16),
        "tp",
        0,
    )
    hidden = normalize(residual.astype(jnp.float32) + mixed_rows, resid_gain).astype(jnp.bfloat16)
    experts = lax.axis_size("sp")
    top_count = expert_ids.shape[1]
    capacity = 2 * own_count * top_count // experts
    width = hidden.shape[1]
    gate_local = w_gate[0]
    up_local = w_up[0]
    down_local = w_down[0]

    def activate(arrived):
        arrived_shape = arrived.shape
        flat_rows = arrived.reshape(-1, arrived_shape[-1])
        activity = expert_activity(flat_rows, gate_local, up_local)
        return activity.reshape(arrived_shape[:-1] + (gate_local.shape[1],))

    own_table, positions = slot_layout(expert_ids, experts, capacity)
    padded = jnp.concatenate([hidden, jnp.zeros((1, width), jnp.bfloat16)], axis=0)
    dispatched = padded[own_table].reshape(experts, capacity, width)
    arrived = lax.all_to_all(dispatched, "sp", split_axis=0, concat_axis=0, tiled=True)

    def activate_piece(slot_piece, first_row):
        return activate(slot_piece)

    activity = work_in_pieces(arrived[None], "tp", 0, activate_piece, 0)
    activity_rows = activity.reshape(-1, activity.shape[-1])
    section = activity_rows
    expert_out = lax.psum_scatter(
        jnp.dot(section, down_local, preferred_element_type=jnp.float32).astype(jnp.bfloat16),
        "tp",
        scatter_dimension=0,
        tiled=True,
    )
    expert_out = expert_out.reshape(experts, capacity, width)
    returned_rows = lax.all_to_all(expert_out, "sp", split_axis=0, concat_axis=0, tiled=True)
    picked = returned_rows.reshape(experts * capacity, width)[positions.reshape(-1)]
    picked = picked.reshape(own_count, top_count, width)
    routed_sum = jnp.einsum("tk,tkd->td", route_weight, picked.astype(jnp.float32))
    return normalize(hidden.astype(jnp.float32) + routed_sum, out_gain).astype(jnp.bfloat16)


def solution(mesh):
    in_specs = (
        P("sp", "tp"),
        P("sp", "tp"),
        P(None, "tp"),
        P("tp"),
        P("tp", None),
        P(("sp", "tp"), None),
        P(),
        P(("sp", "tp"), None),
        P(("sp", "tp"), None),
        P("sp", None, "tp"),
        P("sp", None, "tp"),
        P("sp", "tp", None),
        P(),
    )
    out_specs = P(("sp", "tp"), None)
    return jax.shard_map(shards, mesh=mesh, in_specs=in_specs, out_specs=out_specs, check_vma=False)
```

profile of v0, /device:TPU:1, one launch (start us, length us, event | category | flops | bytes accessed | tf_op | source)
XLA Modules:
  0.0 399.4 jit_solution(7597769521617567499)
XLA Ops:
  6.5 0.0 copy-start
  6.5 1.6 multiply_convert_fusion.4
  8.2 4.6 %collective-permute-start = (bf16[30,512]{1,0:T(8,128)(2,1)S(1)}, bf16[30,512]{1,0:T(8,128)(2,1)S(1)}, u32[]{:S(2)}, u32[]{:S(2)}) collective-permute-start(bf16[30,512]{1,0:T(8,128)(2,1)S(1)} %slice.272), channel_id=1, source_target_pairs={{0,4},{4,8},{8,12},{12,16},{16,20},{20,24},{24,28},{28,32},{32,36}... | collective-permute-start | bytes 92168 | tf_op jit(solution)/shard_map/ppermute | solution.py:17
  12.8 1.1 fusion.49
  13.9 1.1 fusion.50
  15.0 0.0 collective-permute-done
  15.0 0.2 maximum_convert_fusion
  15.2 0.0 copy-start.8
  15.2 5.8 %fusion.47 = (f32[512]{0:T(512)S(1)}, f32[512]{0:T(512)S(1)}, f32[512,512]{1,0:T(8,128)}) fusion(f32[542,512]{1,0:T(8,128)S(1)} %maximum_convert_fusion, f32[512]{0:T(512)S(1)} %bitcast.116, f32[512]{0:T(512)S(1)} %bitcast.117, f32[512]{0:T(512)S(1)} %bitcast.88, f32[512]{0:T(512)S(1)} %bitcast.89, f32[512]{0:T(512)S(1)} %bitcast.90, f32[512]{0:T(512)S(1)} %bitcast.91, ...), kind=kLoop, calls=%fused_computation.116 | loop fusion | flops 16776192 | bytes 33622016 | tf_op jit(solution)/shard_map/reduce_sum | solution.py:119
  21.0 8.0 %all_to_all.21 = f32[4,1,1024]{2,1,0:T(1,128)S(1)} all-to-all(f32[4,1,1024]{2,1,0:T(1,128)S(1)} %broadcast_in_dim.6), channel_id=1, replica_groups=mesh['sp'=64,'tp'=4] {'tp'}, dimensions={0} | all-to-all | bytes 32768 | tf_op jit(solution)/shard_map/all_to_all | solution.py:22
  29.0 0.0 copy-done.8
  29.1 4.7 %convolution_convert_fusion.1 = bf16[512,2048]{1,0:T(8,128)(2,1)} fusion(bf16[512,2048]{1,0:T(8,128)(2,1)} %param.17, f32[512,512]{1,0:T(8,128)} %get-tuple-element.7, f32[512]{0:T(512)S(1)} %copy-done.8, f32[512]{0:T(512)S(1)} %get-tuple-element.40, f32[512]{0:T(512)S(1)} %get-tuple-element.39), kind=kOutput, calls=%fused_computation.6 | convolution fusion | flops 1076887552 | bytes 5249024 | tf_op jit(solution)/shard_map/dot_general | solution.py:129
  33.8 0.0 copy-start.4
  33.8 4.6 %all-to-all-start.1 = ((bf16[4,128,2048]{2,1,0:T(8,128)(2,1)}), bf16[4,128,2048]{2,1,0:T(8,128)(2,1)}, u32[]{:S(2)}, u32[]{:S(2)}) async-start(bf16[4,128,2048]{2,1,0:T(8,128)(2,1)} %bitcast.85), calls=%async_computation.1 | async-start | bytes 4194304 | tf_op jit(solution)/shard_map/all_to_all | solution.py:46
  38.4 0.0 copy-start.1
  38.4 0.0 all-gather.3.cloned.1.call-start
  38.4 0.0 copy-done.4
  38.5 0.1 copy.28
  38.6 0.1 eq.29
  38.7 0.1 eq.25
  38.9 0.6 reduce-window.6
  39.5 0.2 slice_reduce_fusion
  39.7 0.1 copy.27
  39.8 0.1 mul.509
  40.0 0.1 fusion.42
  40.1 1.4 scatter_custom_fusion
  41.5 23.3 %all-to-all-done.1 = bf16[4,128,2048]{2,1,0:T(8,128)(2,1)} async-done(((bf16[4,128,2048]{2,1,0:T(8,128)(2,1)}), bf16[4,128,2048]{2,1,0:T(8,128)(2,1)}, u32[]{:S(2)}, u32[]{:S(2)}) %all-to-all-start.1) | async-done | bytes 2097184 | tf_op jit(solution)/shard_map/all_to_all | solution.py:46
  64.8 2.1 convert_reduce_fusion
  66.9 0.0 copy-done.1
  66.9 0.0 copy-start.2
  66.9 0.2 fusion.38
  67.2 0.3 multiply_reduce_fusion.1
  67.5 0.2 copy-done.2
  67.6 0.3 multiply_convert_fusion.2
  68.0 3.3 gather_fusion
  71.3 62.1 %all_to_all.22 = bf16[64,8,2048]{2,1,0:T(8,128)(2,1)} all-to-all(bf16[64,8,2048]{2,1,0:T(8,128)(2,1)} %bitcast.84), channel_id=1, replica_groups=mesh['sp'=64,'tp'=4] {'sp'}, dimensions={0} | all-to-all | bytes 4194304 | tf_op jit(solution)/shard_map/all_to_all | solution.py:151
  133.4 0.0 all-gather.3.cloned.1.call-update
  133.4 0.2 reduce-scatter.2.cloned.1.call-start
  133.6 81.1 %all-gather.3.cloned.1.call-done = bf16[256,8,2048]{2,1,0:T(8,128)(2,1)} async-done(((bf16[64,8,2048]{2,1,0:T(8,128)(2,1)}), bf16[256,8,2048]{2,1,0:T(8,128)(2,1)}) %all-gather.3.cloned.1.call-update) | async-done | bytes 8388624 | tf_op jit(solution)/shard_map/all_gather | solution.py:63
  214.7 0.0 copy-start.6
  214.7 0.0 copy-start.7
  214.7 7.7 %fusion.2 = f32[4,512,512]{2,1,0:T(8,128)S(1)} fusion(bf16[4,512,2048]{2,1,0:T(8,128)(2,1)} %bitcast.122, bf16[1,2048,512]{2,1,0:T(8,128)(2,1)} %param.23), kind=kOutput, calls=%fused_computation.9 | convolution fusion | flops 4294967296 | bytes 14680064 | tf_op jit(solution)/shard_map/vmap()/dot_general | solution.py:87
  222.4 0.0 copy-done.6
  222.4 0.0 copy-done.7
  222.5 5.7 %multiply_convert_fusion = bf16[4,512,512]{2,1,0:T(8,128)(2,1)S(1)} fusion(f32[4,512,512]{2,1,0:T(8,128)S(1)} %fusion.2, bf16[4,512,2048]{2,1,0:T(8,128)(2,1)S(1)} %bitcast.123, bf16[1,2048,512]{2,1,0:T(8,128)(2,1)S(1)} %copy-done.7), kind=kOutput, calls=%fused_computation.4 | convolution fusion | flops 4305453056 | bytes 16777216 | tf_op jit(solution)/shard_map/vmap()/dot_general | solution.py:86
  228.2 0.0 copy-done
  228.2 6.8 %convolution_convert_fusion = bf16[2048,2048]{1,0:T(8,128)(2,1)} fusion(bf16[2048,512]{1,0:T(8,128)(2,1)S(1)} %bitcast.124, bf16[1,512,2048]{2,1,0:T(8,128)(2,1)S(1)} %copy-done), kind=kOutput, calls=%fused_computation.3 | convolution fusion | flops 4299161600 | bytes 12582912 | tf_op jit(solution)/shard_map/dot_general | solution.py:160
  235.0 0.0 reduce-scatter.2.cloned.1.call-update
  235.0 84.3 %reduce-scatter.2.cloned.1.call-done = bf16[512,2048]{1,0:T(8,128)(2,1)} async-done(((bf16[2048,2048]{1,0:T(8,128)(2,1)}), bf16[512,2048]{1,0:T(8,128)(2,1)}) %reduce-scatter.2.cloned.1.call-update) | async-done | bytes 2097168 | tf_op jit(solution)/shard_map/reduce_scatter | solution.py:159
  319.3 0.0 copy-start.5
  319.3 11.1 %all-to-all-start.3 = ((bf16[64,8,2048]{2,1,0:T(8,128)(2,1)}), bf16[64,8,2048]{2,1,0:T(8,128)(2,1)}, u32[]{:S(2)}, u32[]{:S(2)}) async-start(bf16[64,8,2048]{2,1,0:T(8,128)(2,1)} %bitcast.86), calls=%async_computation.4 | async-start | bytes 4194304 | tf_op jit(solution)/shard_map/all_to_all | solution.py:166
  330.4 0.0 copy-done.5
  330.4 0.2 copy.31
  330.6 49.4 %all-to-all-done.3 = bf16[64,8,2048]{2,1,0:T(8,128)(2,1)} async-done(((bf16[64,8,2048]{2,1,0:T(8,128)(2,1)}), bf16[64,8,2048]{2,1,0:T(8,128)(2,1)}, u32[]{:S(2)}, u32[]{:S(2)}) %all-to-all-start.3) | async-done | bytes 2097184 | tf_op jit(solution)/shard_map/all_to_all | solution.py:166
  380.0 5.2 %gather_fusion.1 = bf16[256,2048]{1,0:T(8,128)(2,1)} fusion(bf16[512,2048]{1,0:T(8,128)(2,1)} %bitcast.44, s32[1024]{0:T(1024)S(1)} %pad_clamp_fusion), kind=kCustom, calls=%fused_computation.1 | custom fusion | bytes 2098176 | tf_op jit(solution)/shard_map/gather | solution.py:167
  385.2 2.5 reshape.111
  387.7 2.5 fusion.51
  390.2 0.0 copy-start.3
  390.2 0.6 fusion.39
  390.8 0.4 multiply_reduce_fusion
  391.2 0.0 copy-done.3
  391.2 1.3 multiply_convert_fusion.1
  (19 shorter events, 0.2 us)
Async XLA Ops:
  6.5 221.6 %copy-start = (bf16[1,512,2048]{2,1,0:T(8,128)(2,1)S(1)}, bf16[1,512,2048]{2,1,0:T(8,128)(2,1)}, u32[]{:S(2)}) copy-start(bf16[1,512,2048]{2,1,0:T(8,128)(2,1)} %param.24) | copy-start | bytes 6291460
  8.2 6.8 %collective-permute-start = (bf16[30,512]{1,0:T(8,128)(2,1)S(1)}, bf16[30,512]{1,0:T(8,128)(2,1)S(1)}, u32[]{:S(2)}, u32[]{:S(2)}) collective-permute-start(bf16[30,512]{1,0:T(8,128)(2,1)S(1)} %slice.272), channel_id=1, source_target_pairs={{0,4},{4,8},{8,12},{12,16},{16,20},{20,24},{24,28},{28,32},{32,36}... | collective-permute-start | bytes 92168 | tf_op jit(solution)/shard_map/ppermute | solution.py:17
  15.2 13.9 %copy-start.8 = (f32[512]{0:T(512)S(1)}, f32[512]{0:T(512)}, u32[]{:S(2)}) copy-start(f32[512]{0:T(512)} %param.16) | copy-start | bytes 6148
  33.8 4.7 %copy-start.4 = (s32[128,2]{0,1:T(2,128)S(1)}, s32[128,2]{0,1:T(2,128)}, u32[]{:S(2)}) copy-start(s32[128,2]{0,1:T(2,128)} %param.20) | copy-start | bytes 3076
  33.8 31.0 %all-to-all-start.1 = ((bf16[4,128,2048]{2,1,0:T(8,128)(2,1)}), bf16[4,128,2048]{2,1,0:T(8,128)(2,1)}, u32[]{:S(2)}, u32[]{:S(2)}) async-start(bf16[4,128,2048]{2,1,0:T(8,128)(2,1)} %bitcast.85), calls=%async_computation.1 | async-start | bytes 4194304 | tf_op jit(solution)/shard_map/all_to_all | solution.py:46
  38.4 28.5 %copy-start.1 = (bf16[128,2048]{1,0:T(8,128)(2,1)S(1)}, bf16[128,2048]{1,0:T(8,128)(2,1)}, u32[]{:S(2)}) copy-start(bf16[128,2048]{1,0:T(8,128)(2,1)} %param.18) | copy-start | bytes 1572868
  38.4 176.3 %all-gather.3.cloned.1.call-start = ((), (), s32[]{:S(2)}) async-start(), calls=%async_computation.6 | async-start | bytes 10485760 | tf_op jit(solution)/shard_map/all_gather | solution.py:63
  66.9 0.7 copy-start.2
  133.4 185.9 %reduce-scatter.2.cloned.1.call-start = ((), (), s32[]{:S(2)}) async-start(), calls=%async_computation.5 | async-start | bytes 10485760 | tf_op jit(solution)/shard_map/reduce_scatter | solution.py:159
  214.7 7.7 %copy-start.6 = (bf16[256,8,2048]{2,1,0:T(8,128)(2,1)S(1)}, bf16[256,8,2048]{2,1,0:T(8,128)(2,1)}, u32[]{:S(2)}) copy-start(bf16[256,8,2048]{2,1,0:T(8,128)(2,1)} %all-gather.3.cloned.1.call-done) | copy-start | bytes 25165828
  214.7 7.7 %copy-start.7 = (bf16[1,2048,512]{2,1,0:T(8,128)(2,1)S(1)}, bf16[1,2048,512]{2,1,0:T(8,128)(2,1)}, u32[]{:S(2)}) copy-start(bf16[1,2048,512]{2,1,0:T(8,128)(2,1)} %param.22) | copy-start | bytes 6291460
  319.3 11.1 %copy-start.5 = (f32[128,2]{0,1:T(2,128)S(1)}, f32[128,2]{0,1:T(2,128)}, u32[]{:S(2)}) copy-start(f32[128,2]{0,1:T(2,128)} %param.21) | copy-start | bytes 3076
  319.3 60.7 %all-to-all-start.3 = ((bf16[64,8,2048]{2,1,0:T(8,128)(2,1)}), bf16[64,8,2048]{2,1,0:T(8,128)(2,1)}, u32[]{:S(2)}, u32[]{:S(2)}) async-start(bf16[64,8,2048]{2,1,0:T(8,128)(2,1)} %bitcast.86), calls=%async_computation.4 | async-start | bytes 4194304 | tf_op jit(solution)/shard_map/all_to_all | solution.py:166
  390.2 1.0 copy-start.3
Sparse Core Ops, SparseCore 0:
  133.5 81.1 all-gather.2
  235.1 84.1 reduce-scatter.1
where the time goes:
time: 401 us; the launch traced here: 399 us
  waiting for transfers between devices  238 us (59%)
  blocking collectives  70.1 us (17%)
  matrix products  27.4 us (7%)
  starting transfers between devices  20.5 us (5%)
  local copies, waits for them, and re-layouts  15.9 us (4%)
  other arithmetic  13.7 us (3%)
  between operations  13.7 us (3%)
    reduce_scatter x1, waiting for transfers between devices, shards(): lax.psum_scatter(jnp.dot(section, down_local, preferred_element_type=jnp....  84.3 us
    all_gather x1, waiting for transfers between devices, work_in_pieces(): done.append(jax.vmap(apply)(lax.all_gather(section, axis), starts))  81.1 us
    all_to_all x1, blocking collectives, shards(): lax.all_to_all(dispatched, 'sp', split_axis=0, concat_axis=0, tiled=True)  62.1 us
    all_to_all x1, waiting for transfers between devices, shards(): lax.all_to_all(expert_out, 'sp', split_axis=0, concat_axis=0, tiled=True)  49.4 us
    all_to_all x1, waiting for transfers between devices, sum_at_owner(): lax.all_to_all(tiles, axis, split_axis=0, concat_axis=0, tiled=True)  23.3 us
    all_to_all x1, starting transfers between devices, shards(): lax.all_to_all(expert_out, 'sp', split_axis=0, concat_axis=0, tiled=True)  11.1 us
    all_to_all x1, blocking collectives, copy_for_each(): lax.all_to_all(jnp.broadcast_to(array[None], (count, *array.shape)), axis...  8.03 us
  transfers between devices with their start and end apart: 5, of which 4 were waited for; matrix products, arithmetic and copies ran while one was open for 1% of the time, Pallas kernels for 0%

commit v1 on v0

--- a/solution.py
+++ b/solution.py
@@ -68,6 +68,24 @@
     centre = jnp.mean(values, axis=-1, keepdims=True)
     spread = jnp.mean(jnp.square(values - centre), axis=-1, keepdims=True)
     return (values - centre) * lax.rsqrt(spread + EPSILON) * gain_vector
+
+
+def swap_route(nearby):
+    count, size = (lax.axis_size("sp"), lax.axis_size("tp"))
+    route = []
+    for s in range(count):
+        for t in range(size):
+            partner = t ^ 1 if (s % 2 == 0) == nearby else size - 1 - t
+            route.append((s * size + t, s * size + partner))
+    return route
+
+
+def weight_route():
+    return swap_route(True)
+
+
+def cross_route():
+    return swap_route(False)
 
 
 def slot_layout(route_ids, experts, capacity):
@@ -139,29 +157,27 @@
     up_local = w_up[0]
     down_local = w_down[0]
 
-    def activate(arrived):
-        arrived_shape = arrived.shape
-        flat_rows = arrived.reshape(-1, arrived_shape[-1])
-        activity = expert_activity(flat_rows, gate_local, up_local)
-        return activity.reshape(arrived_shape[:-1] + (gate_local.shape[1],))
+    gate_other, up_other, down_other = (
+        lax.ppermute(w, ("sp", "tp"), weight_route()) for w in (gate_local, up_local, down_local)
+    )
+
+    def half_experts(rows):
+        own = expert_activity(rows, gate_local, up_local)
+        other = expert_activity(rows, gate_other, up_other)
+        return jnp.dot(own, down_local, preferred_element_type=jnp.float32) + jnp.dot(
+            other, down_other, preferred_element_type=jnp.float32
+        )
 
     own_table, positions = slot_layout(expert_ids, experts, capacity)
     padded = jnp.concatenate([hidden, jnp.zeros((1, width), jnp.bfloat16)], axis=0)
     dispatched = padded[own_table].reshape(experts, capacity, width)
     arrived = lax.all_to_all(dispatched, "sp", split_axis=0, concat_axis=0, tiled=True)
-
-    def activate_piece(slot_piece, first_row):
-        return activate(slot_piece)
-
-    activity = work_in_pieces(arrived[None], "tp", 0, activate_piece, 0)
-    activity_rows = activity.reshape(-1, activity.shape[-1])
-    section = activity_rows
-    expert_out = lax.psum_scatter(
-        jnp.dot(section, down_local, preferred_element_type=jnp.float32).astype(jnp.bfloat16),
-        "tp",
-        scatter_dimension=0,
-        tiled=True,
-    )
+    arrived = arrived.reshape(experts * capacity, width)
+    crossed = lax.ppermute(arrived, ("sp", "tp"), cross_route())
+    sent = half_experts(crossed)
+    kept = half_experts(arrived)
+    back = lax.ppermute(sent.astype(jnp.bfloat16), ("sp", "tp"), cross_route())
+    expert_out = (kept + back.astype(jnp.float32)).astype(jnp.bfloat16)
     expert_out = expert_out.reshape(experts, capacity, width)
     returned_rows = lax.all_to_all(expert_out, "sp", split_axis=0, concat_axis=0, tiled=True)
     picked = returned_rows.reshape(experts * capacity, width)[positions.reshape(-1)]

time: 401 us -> 333 us (0.83)
  waiting for transfers between devices: 238 us -> 153 us
  matrix products: 27.4 us -> 48.8 us
  between operations: 13.7 us -> 0.28 us
  other arithmetic: 13.7 us -> 20.3 us
    reduce_scatter x1 -> x0, waiting for transfers between devices: 84.3 us -> none  [shards(): lax.psum_scatter(jnp.dot(section, down_local, preferred_element_type=jnp....]
    all_gather x1 -> x0, waiting for transfers between devices: 81.1 us -> none  [work_in_pieces(): done.append(jax.vmap(apply)(lax.all_gather(section, axis), starts))]
    ppermute x0 -> x5, waiting for transfers between devices: none -> 80.4 us  [the longest x1 40.4 us: shards(): crossed = lax.ppermute(arrived, ('sp', 'tp'), cross_route())]
    dot_general x2 -> x4, matrix products: 14.5 us -> 30.9 us  [the longest x2 15.8 us: half_experts(): jnp.dot(other, down_other, preferred_element_type=jnp.float32)]
    reshape x0 -> x1, other arithmetic: none -> 6.66 us  [shards(): expert_out = expert_out.reshape(experts, capacity, width)]
    dot_general x1 -> x4, matrix products: 5.72 us -> 11.3 us  [expert_activity(): gate_pre = jnp.dot(tokens, gate_matrix, preferred_element_type=jnp.float32)]
  transfers between devices with their start and end apart: 5 -> 8, of which waited for: 4 -> 7; matrix products, arithmetic and copies ran while one was open for 1% -> 12% of each run, Pallas kernels for 0% -> 0%
where the time goes in v1:
time: 333 us; the launch traced here: 332 us
  waiting for transfers between devices  153 us (46%)
  blocking collectives  70.2 us (21%)
  matrix products  48.8 us (15%)
  starting transfers between devices  20.7 us (6%)
  other arithmetic  20.3 us (6%)
  local copies, waits for them, and re-layouts  18.6 us (6%)
    all_to_all x1, blocking collectives, shards(): lax.all_to_all(dispatched, 'sp', split_axis=0, concat_axis=0, tiled=True)  62.1 us
    all_to_all x1, waiting for transfers between devices, shards(): lax.all_to_all(expert_out, 'sp', split_axis=0, concat_axis=0, tiled=True)  49.4 us
    ppermute x1, waiting for transfers between devices, shards(): crossed = lax.ppermute(arrived, ('sp', 'tp'), cross_route())  40.4 us
    ppermute x3, waiting for transfers between devices, shards(): lax.ppermute(w, ('sp', 'tp'), weight_route())  36.6 us
    all_to_all x1, waiting for transfers between devices, sum_at_owner(): lax.all_to_all(tiles, axis, split_axis=0, concat_axis=0, tiled=True)  23.3 us
    dot_general x2, matrix products, half_experts(): jnp.dot(other, down_other, preferred_element_type=jnp.float32)  15.8 us
    dot_general x2, matrix products, half_experts(): jnp.dot(own, down_local, preferred_element_type=jnp.float32)  15.1 us
    dot_general x4, matrix products, expert_activity(): gate_pre = jnp.dot(tokens, gate_matrix, preferred_element_type=jnp.float32)  11.3 us
  transfers between devices with their start and end apart: 8, of which 7 were waited for; matrix products, arithmetic and copies ran while one was open for 12% of the time, Pallas kernels for 0%

profile of v1, /device:TPU:1, one launch (start us, length us, event | category | flops | bytes accessed | tf_op | source)
XLA Modules:
  0.0 332.0 jit_solution(16971111654107013844)
XLA Ops:
  0.0 1.6 multiply_convert_fusion.3
  1.7 4.6 %collective-permute-start = (bf16[30,512]{1,0:T(8,128)(2,1)S(1)}, bf16[30,512]{1,0:T(8,128)(2,1)S(1)}, u32[]{:S(2)}, u32[]{:S(2)}) collective-permute-start(bf16[30,512]{1,0:T(8,128)(2,1)S(1)} %slice.272), channel_id=1, source_target_pairs={{0,4},{4,8},{8,12},{12,16},{16,20},{20,24},{24,28},{28,32},{32,36}... | collective-permute-start | bytes 92168 | tf_op jit(solution)/shard_map/ppermute | solution.py:17
  6.3 1.2 fusion.111
  7.4 1.0 fusion.112
  8.4 0.0 collective-permute-done
  8.5 0.2 maximum_convert_fusion
  8.6 0.0 copy-start.12
  8.6 5.8 %fusion.109 = (f32[512]{0:T(512)S(1)}, f32[512]{0:T(512)S(1)}, f32[512,512]{1,0:T(8,128)}) fusion(f32[542,512]{1,0:T(8,128)S(1)} %maximum_convert_fusion, f32[512]{0:T(512)S(1)} %bitcast.139, f32[512]{0:T(512)S(1)} %bitcast.140, f32[512]{0:T(512)S(1)} %bitcast.111, f32[512]{0:T(512)S(1)} %bitcast.112, f32[512]{0:T(512)S(1)} %bitcast.113, ...), kind=kLoop, calls=%fused_computation.182 | loop fusion | flops 16776192 | bytes 33622016 | tf_op jit(solution)/shard_map/reduce_sum | solution.py:137
  14.4 8.0 %all_to_all.21 = f32[4,1,1024]{2,1,0:T(1,128)S(1)} all-to-all(f32[4,1,1024]{2,1,0:T(1,128)S(1)} %broadcast_in_dim.6), channel_id=1, replica_groups=mesh['sp'=64,'tp'=4] {'tp'}, dimensions={0} | all-to-all | bytes 32768 | tf_op jit(solution)/shard_map/all_to_all | solution.py:22
  22.5 4.0 %convolution_convert_fusion = bf16[512,2048]{1,0:T(8,128)(2,1)} fusion(bf16[512,2048]{1,0:T(8,128)(2,1)S(1)} %copy-done, f32[512,512]{1,0:T(8,128)} %get-tuple-element.7, f32[512]{0:T(512)S(1)} %copy-done.12, f32[512]{0:T(512)S(1)} %get-tuple-element.40, f32[512]{0:T(512)S(1)} %get-tuple-element.39), kind=kOutput, calls=%fused_computation.6 | convolution fusion | flops 1076887552 | bytes 5249024 | tf_op jit(solution)/shard_map/dot_general | solution.py:147
  26.5 4.6 %all-to-all-start.1 = ((bf16[4,128,2048]{2,1,0:T(8,128)(2,1)}), bf16[4,128,2048]{2,1,0:T(8,128)(2,1)}, u32[]{:S(2)}, u32[]{:S(2)}) async-start(bf16[4,128,2048]{2,1,0:T(8,128)(2,1)} %bitcast.109), calls=%async_computation.1 | async-start | bytes 4194304 | tf_op jit(solution)/shard_map/all_to_all | solution.py:46
  31.1 0.0 copy-start.1
  31.2 0.1 copy.24
  31.3 0.1 eq.25
  31.4 0.1 eq.29
  31.6 0.1 copy.23
  31.7 0.1 mul.533
  31.8 0.6 reduce-window.6
  32.4 0.2 slice_reduce_fusion
  32.7 0.1 fusion.74
  32.8 1.4 scatter_custom_fusion
  34.2 23.3 %all-to-all-done.1 = bf16[4,128,2048]{2,1,0:T(8,128)(2,1)} async-done(((bf16[4,128,2048]{2,1,0:T(8,128)(2,1)}), bf16[4,128,2048]{2,1,0:T(8,128)(2,1)}, u32[]{:S(2)}, u32[]{:S(2)}) %all-to-all-start.1) | async-done | bytes 2097184 | tf_op jit(solution)/shard_map/all_to_all | solution.py:46
  57.5 2.1 convert_reduce_fusion
  59.7 0.0 copy-start.4
  59.7 0.2 fusion.70
  59.9 0.3 multiply_reduce_fusion.1
  60.2 0.2 copy-done.4
  60.4 0.3 multiply_convert_fusion.1
  60.7 3.3 %gather_fusion = bf16[512,2048]{1,0:T(8,128)(2,1)} fusion(bf16[129,2048]{1,0:T(8,128)(2,1)S(1)} %concatenate.11, s32[1024]{0:T(1024)S(1)} %pad_clamp_fusion.1), kind=kCustom, calls=%fused_computation | custom fusion | bytes 4196352 | tf_op jit(solution)/shard_map/gather | solution.py:173
  64.0 62.1 %all_to_all.22 = bf16[64,8,2048]{2,1,0:T(8,128)(2,1)S(1)} all-to-all(bf16[64,8,2048]{2,1,0:T(8,128)(2,1)} %bitcast.107), channel_id=1, replica_groups=mesh['sp'=64,'tp'=4] {'sp'}, dimensions={0} | all-to-all | bytes 4194304 | tf_op jit(solution)/shard_map/all_to_all | solution.py:174
  126.2 1.4 copy-done.2
  127.5 0.3 collective-permute-start.4
  127.8 0.6 collective-permute-start.2
  128.4 2.1 collective-permute-start.3
  130.5 0.6 collective-permute-start.1
  131.1 40.4 %collective-permute-done.4 = bf16[512,2048]{1,0:T(8,128)(2,1)S(1)} collective-permute-done((bf16[512,2048]{1,0:T(8,128)(2,1)S(1)}, bf16[512,2048]{1,0:T(8,128)(2,1)S(1)}, u32[]{:S(2)}, u32[]{:S(2)}) %collective-permute-start.4) | collective-permute-done | bytes 2097184 | tf_op jit(solution)/shard_map/ppermute | solution.py:176
  171.5 2.2 convolution_minimum_fusion.1
  173.7 0.7 collective-permute-done.2
  174.4 0.0 copy-done.11
  174.4 1.3 copy-done.9
  175.8 2.2 convolution_minimum_fusion
  178.0 7.6 %fusion.49 = f32[512,2048]{1,0:T(8,128)} fusion(f32[512,512]{1,0:T(8,128)} %convolution_minimum_fusion.1, bf16[512,2048]{1,0:T(8,128)(2,1)} %copy-done.11, bf16[1,512,2048]{2,1,0:T(8,128)(2,1)} %param.24, bf16[1,2048,512]{2,1,0:T(8,128)(2,1)} %param.23), kind=kOutput, calls=%fused_computation.104 | convolution fusion | flops 2149842944 | bytes 11534336 | tf_op jit(solution)/shard_map/dot_general | solution.py:167
  185.6 13.4 %collective-permute-done.3 = bf16[512,2048]{1,0:T(8,128)(2,1)} collective-permute-done((bf16[512,2048]{1,0:T(8,128)(2,1)}, bf16[512,2048]{1,0:T(8,128)(2,1)}, u32[]{:S(2)}, u32[]{:S(2)}) %collective-permute-start.3) | collective-permute-done | bytes 2097184 | tf_op jit(solution)/shard_map/ppermute | solution.py:161
  199.0 22.5 %collective-permute-done.1 = bf16[2048,512]{1,0:T(8,128)(2,1)} collective-permute-done((bf16[2048,512]{1,0:T(8,128)(2,1)}, bf16[2048,512]{1,0:T(8,128)(2,1)}, u32[]{:S(2)}, u32[]{:S(2)}) %collective-permute-start.1) | collective-permute-done | bytes 2097184 | tf_op jit(solution)/shard_map/ppermute | solution.py:161
  221.4 8.2 %add_convert_fusion.1 = bf16[512,2048]{1,0:T(8,128)(2,1)} fusion(f32[512,2048]{1,0:T(8,128)} %fusion.49, bf16[512,2048]{1,0:T(8,128)(2,1)} %collective-permute-done.3, f32[512,512]{1,0:T(8,128)} %convolution_minimum_fusion, bf16[512,2048]{1,0:T(8,128)(2,1)} %copy-done.11, bf16[2048,512]{1,0:T(8,128)(2,1)} %collective-permute-done.1), kind=kOutput, calls=%fused_computation.4 | convolution fusion | flops 2151940096 | bytes 13631488 | tf_op jit(solution)/shard_map/dot_general | solution.py:167
  229.6 0.0 collective-permute-start.5
  229.6 4.6 %convolution_minimum_fusion.3 = f32[512,512]{1,0:T(8,128)} fusion(bf16[1,2048,512]{2,1,0:T(8,128)(2,1)} %param.22, bf16[64,8,2048]{2,1,0:T(8,128)(2,1)} %copy-done.2), kind=kOutput, calls=%fused_computation.14 | convolution fusion | flops 1074003968 | bytes 5242880 | tf_op jit(solution)/shard_map/dot_general | solution.py:104
  234.3 0.0 copy-done.10
  234.3 2.2 convolution_minimum_fusion.2
  236.5 7.6 %fusion.47 = f32[512,2048]{1,0:T(8,128)} fusion(f32[512,512]{1,0:T(8,128)} %convolution_minimum_fusion.3, bf16[1,512,2048]{2,1,0:T(8,128)(2,1)} %param.24, bf16[1,2048,512]{2,1,0:T(8,128)(2,1)} %param.23, bf16[64,8,2048]{2,1,0:T(8,128)(2,1)} %copy-done.2), kind=kOutput, calls=%fused_computation.102 | convolution fusion | flops 2149842944 | bytes 11534336 | tf_op jit(solution)/shard_map/dot_general | solution.py:167
  244.1 7.6 %fusion.48 = f32[512,2048]{1,0:T(8,128)} fusion(bf16[512,2048]{1,0:T(8,128)(2,1)} %collective-permute-done.3, f32[512,512]{1,0:T(8,128)} %convolution_minimum_fusion.2, bf16[2048,512]{1,0:T(8,128)(2,1)} %collective-permute-done.1, bf16[64,8,2048]{2,1,0:T(8,128)(2,1)} %copy-done.2), kind=kOutput, calls=%fused_computation.103 | convolution fusion | flops 2149842944 | bytes 11534336 | tf_op jit(solution)/shard_map/dot_general | solution.py:167
  251.7 3.4 %collective-permute-done.5 = bf16[512,2048]{1,0:T(8,128)(2,1)} collective-permute-done((bf16[512,2048]{1,0:T(8,128)(2,1)}, bf16[512,2048]{1,0:T(8,128)(2,1)}, u32[]{:S(2)}, u32[]{:S(2)}) %collective-permute-start.5) | collective-permute-done | bytes 2097184 | tf_op jit(solution)/shard_map/ppermute | solution.py:179
  255.1 6.7 %fusion = bf16[64,8,2048]{2,1,0:T(8,128)(2,1)} fusion(bf16[512,2048]{1,0:T(8,128)(2,1)} %collective-permute-done.5, f32[512,2048]{1,0:T(8,128)} %fusion.47, f32[512,2048]{1,0:T(8,128)} %fusion.48), kind=kLoop, calls=%fused_computation.7 | loop fusion | flops 4194304 | bytes 12582912 | tf_op jit(solution)/shard_map/reshape | solution.py:181
  261.8 8.0 %all-to-all-start.3 = ((bf16[64,8,2048]{2,1,0:T(8,128)(2,1)}), bf16[64,8,2048]{2,1,0:T(8,128)(2,1)}, u32[]{:S(2)}, u32[]{:S(2)}) async-start(bf16[64,8,2048]{2,1,0:T(8,128)(2,1)} %fusion), calls=%async_computation.3 | async-start | bytes 4194304 | tf_op jit(solution)/shard_map/all_to_all | solution.py:182
  269.8 0.0 copy-done.7
  269.8 0.2 copy.27
  269.9 49.4 %all-to-all-done.3 = bf16[64,8,2048]{2,1,0:T(8,128)(2,1)} async-done(((bf16[64,8,2048]{2,1,0:T(8,128)(2,1)}), bf16[64,8,2048]{2,1,0:T(8,128)(2,1)}, u32[]{:S(2)}, u32[]{:S(2)}) %all-to-all-start.3) | async-done | bytes 2097184 | tf_op jit(solution)/shard_map/all_to_all | solution.py:182
  319.4 5.2 %gather_fusion.1 = bf16[256,2048]{1,0:T(8,128)(2,1)} fusion(bf16[512,2048]{1,0:T(8,128)(2,1)} %bitcast.41, s32[1024]{0:T(1024)S(1)} %pad_clamp_fusion), kind=kCustom, calls=%fused_computation.1 | custom fusion | bytes 2098176 | tf_op jit(solution)/shard_map/gather | solution.py:183
  324.6 2.5 reshape.107
  327.1 2.5 fusion.113
  329.6 0.0 copy-start.5
  329.6 0.6 fusion.71
  330.2 0.4 multiply_reduce_fusion
  330.6 1.3 multiply_convert_fusion
  (35 shorter events, 0.3 us)
Async XLA Ops:
  0.0 22.5 %copy-start = (bf16[512,2048]{1,0:T(8,128)(2,1)S(1)}, bf16[512,2048]{1,0:T(8,128)(2,1)}, u32[]{:S(2)}) copy-start(bf16[512,2048]{1,0:T(8,128)(2,1)} %param.17) | copy-start | bytes 6291460
  1.7 6.8 %collective-permute-start = (bf16[30,512]{1,0:T(8,128)(2,1)S(1)}, bf16[30,512]{1,0:T(8,128)(2,1)S(1)}, u32[]{:S(2)}, u32[]{:S(2)}) collective-permute-start(bf16[30,512]{1,0:T(8,128)(2,1)S(1)} %slice.272), channel_id=1, source_target_pairs={{0,4},{4,8},{8,12},{12,16},{16,20},{20,24},{24,28},{28,32},{32,36}... | collective-permute-start | bytes 92168 | tf_op jit(solution)/shard_map/ppermute | solution.py:17
  8.6 13.9 %copy-start.12 = (f32[512]{0:T(512)S(1)}, f32[512]{0:T(512)}, u32[]{:S(2)}) copy-start(f32[512]{0:T(512)} %param.16) | copy-start | bytes 6148
  26.5 4.6 %copy-start.6 = (s32[128,2]{0,1:T(2,128)S(1)}, s32[128,2]{0,1:T(2,128)}, u32[]{:S(2)}) copy-start(s32[128,2]{0,1:T(2,128)} %param.20) | copy-start | bytes 3076
  26.5 31.0 %all-to-all-start.1 = ((bf16[4,128,2048]{2,1,0:T(8,128)(2,1)}), bf16[4,128,2048]{2,1,0:T(8,128)(2,1)}, u32[]{:S(2)}, u32[]{:S(2)}) async-start(bf16[4,128,2048]{2,1,0:T(8,128)(2,1)} %bitcast.109), calls=%async_computation.1 | async-start | bytes 4194304 | tf_op jit(solution)/shard_map/all_to_all | solution.py:46
  31.1 28.5 %copy-start.1 = (bf16[128,2048]{1,0:T(8,128)(2,1)S(1)}, bf16[128,2048]{1,0:T(8,128)(2,1)}, u32[]{:S(2)}) copy-start(bf16[128,2048]{1,0:T(8,128)(2,1)} %param.18) | copy-start | bytes 1572868
  59.7 0.7 copy-start.4
  64.0 63.8 %copy-start.8 = (bf16[1,2048,512]{2,1,0:T(8,128)(2,1)S(1)}, bf16[1,2048,512]{2,1,0:T(8,128)(2,1)}, u32[]{:S(2)}) copy-start(bf16[1,2048,512]{2,1,0:T(8,128)(2,1)} %param.22) | copy-start | bytes 6291460
  126.2 1.4 copy-start.2
  127.5 43.9 %collective-permute-start.4 = (bf16[512,2048]{1,0:T(8,128)(2,1)S(1)}, bf16[512,2048]{1,0:T(8,128)(2,1)S(1)}, u32[]{:S(2)}, u32[]{:S(2)}) collective-permute-start(bf16[512,2048]{1,0:T(8,128)(2,1)S(1)} %bitcast.108), channel_id=1, source_target_pairs={{0,3},{1,2},{2,1},{3,0},{4,5},{5,4},{6,7},{7,6},{8,11},{9,10},{10,... | collective-permute-start | bytes 6291464 | tf_op jit(solution)/shard_map/ppermute | solution.py:176
  127.8 46.6 %collective-permute-start.2 = (bf16[2048,512]{1,0:T(8,128)(2,1)S(1)}, bf16[2048,512]{1,0:T(8,128)(2,1)S(1)}, u32[]{:S(2)}, u32[]{:S(2)}) collective-permute-start(bf16[2048,512]{1,0:T(8,128)(2,1)S(1)} %bitcast.145), channel_id=1, source_target_pairs={{0,1},{1,0},{2,3},{3,2},{4,7},{5,6},{6,5},{7,4},{8,9},{9,8},{10,11... | collective-permute-start | bytes 6291464 | tf_op jit(solution)/shard_map/ppermute | solution.py:161
  128.4 70.5 %collective-permute-start.3 = (bf16[512,2048]{1,0:T(8,128)(2,1)}, bf16[512,2048]{1,0:T(8,128)(2,1)}, u32[]{:S(2)}, u32[]{:S(2)}) collective-permute-start(bf16[512,2048]{1,0:T(8,128)(2,1)} %bitcast.39), channel_id=1, source_target_pairs={{0,1},{1,0},{2,3},{3,2},{4,7},{5,6},{6,5},{7,4},{8,9},{9,8},{10,11... | collective-permute-start | bytes 6291464 | tf_op jit(solution)/shard_map/ppermute | solution.py:161
  130.5 90.9 %collective-permute-start.1 = (bf16[2048,512]{1,0:T(8,128)(2,1)}, bf16[2048,512]{1,0:T(8,128)(2,1)}, u32[]{:S(2)}, u32[]{:S(2)}) collective-permute-start(bf16[2048,512]{1,0:T(8,128)(2,1)} %bitcast.37), channel_id=1, source_target_pairs={{0,1},{1,0},{2,3},{3,2},{4,7},{5,6},{6,5},{7,4},{8,9},{9,8},{10,11... | collective-permute-start | bytes 6291464 | tf_op jit(solution)/shard_map/ppermute | solution.py:161
  171.5 3.0 copy-start.11
  174.4 1.3 copy-start.9
  229.6 4.6 %copy-start.3 = (bf16[64,8,2048]{2,1,0:T(8,128)(2,1)S(1)}, bf16[64,8,2048]{2,1,0:T(8,128)(2,1)}, u32[]{:S(2)}) copy-start(bf16[64,8,2048]{2,1,0:T(8,128)(2,1)} %copy-done.2) | copy-start | bytes 6291460
  229.6 4.6 %copy-start.10 = (bf16[2048,512]{1,0:T(8,128)(2,1)S(1)}, bf16[2048,512]{1,0:T(8,128)(2,1)}, u32[]{:S(2)}) copy-start(bf16[2048,512]{1,0:T(8,128)(2,1)} %copy-done.9) | copy-start | bytes 6291460
  229.6 25.5 %collective-permute-start.5 = (bf16[512,2048]{1,0:T(8,128)(2,1)}, bf16[512,2048]{1,0:T(8,128)(2,1)}, u32[]{:S(2)}, u32[]{:S(2)}) collective-permute-start(bf16[512,2048]{1,0:T(8,128)(2,1)} %add_convert_fusion.1), channel_id=1, source_target_pairs={{0,3},{1,2},{2,1},{3,0},{4,5},{5,4},{6,7},{7,6},{8,11},{9,10},{10,... | collective-permute-start | bytes 6291464 | tf_op jit(solution)/shard_map/ppermute | solution.py:179
  261.8 8.0 %copy-start.7 = (f32[128,2]{0,1:T(2,128)S(1)}, f32[128,2]{0,1:T(2,128)}, u32[]{:S(2)}) copy-start(f32[128,2]{0,1:T(2,128)} %param.21) | copy-start | bytes 3076
  261.8 57.6 %all-to-all-start.3 = ((bf16[64,8,2048]{2,1,0:T(8,128)(2,1)}), bf16[64,8,2048]{2,1,0:T(8,128)(2,1)}, u32[]{:S(2)}, u32[]{:S(2)}) async-start(bf16[64,8,2048]{2,1,0:T(8,128)(2,1)} %fusion), calls=%async_computation.3 | async-start | bytes 4194304 | tf_op jit(solution)/shard_map/all_to_all | solution.py:182
  329.6 1.0 copy-start.5

commit v2 on v0

v2 whole, which is shorter than its diff:
```python
import jax
import jax.numpy as jnp
from jax import lax
from jax.experimental import pallas as pl
from jax.experimental.pallas import tpu as pltpu
from jax.sharding import PartitionSpec as P

DC = 2048


EPSILON = 1e-05
LIMIT = 7.0
SLOPE = 1.702


def shifted(block, axis, distance):
    devices = range(lax.axis_size(axis))
    route = [(i - distance, i) for i in devices if i - distance in devices]
    return lax.ppermute(block, axis, route)


def copy_for_each(array, axis):
    count = lax.axis_size(axis)
    return lax.all_to_all(
        jnp.broadcast_to(array[None], (count, *array.shape)), axis, 0, 0, tiled=True
    )


def of_everyone(array, axis):
    return copy_for_each(array, axis).sum(axis=0)


def together(arrays, axis):
    ends = [0]
    for a in arrays:
        ends.append(ends[-1] + a.size)
    running = of_everyone(jnp.concatenate([a.ravel() for a in arrays]), axis)
    return tuple((running[b:e].reshape(a.shape) for a, b, e in zip(arrays, ends, ends[1:])))


def cut_along(array, dim, count):
    before, after = (array.shape[:dim], array.shape[dim + 1 :])
    return jnp.moveaxis(array.reshape(*before, count, -1, *after), dim, 0)


def sum_at_owner(array, axis, dim):
    tiles = cut_along(array, dim, lax.axis_size(axis))
    arrived = lax.all_to_all(tiles, axis, split_axis=0, concat_axis=0, tiled=True)
    return arrived.astype(jnp.float32).sum(axis=0)


def in_order(tiles, dim):
    dims = list(tiles.shape[1:])
    dims[dim] *= tiles.shape[0]
    return jnp.moveaxis(tiles, 0, dim).reshape(dims)


def normalize(values, gain_vector):
    centre = jnp.mean(values, axis=-1, keepdims=True)
    spread = jnp.mean(jnp.square(values - centre), axis=-1, keepdims=True)
    return (values - centre) * lax.rsqrt(spread + EPSILON) * gain_vector


Z, Y, CORES = 8, 4, 2
PLANE = Y * CORES
GROUPS = 4
PEERS = 2 * PLANE
SELF = 3 * PEERS + PLANE
CAP = 8
TILE = 256
MESH = pl.DeviceIdType.MESH


def position():
    sp, tp = lax.axis_index("sp"), lax.axis_index("tp")
    z, y, core = sp // PLANE, (sp // CORES) % Y, sp % CORES
    near, far = tp + 1 - 2 * (tp % 2), 3 - tp
    weight_partner = near * (1 - core) + far * core
    row_partner = near * core + far * (1 - core)
    return sp, tp, z, y, core, weight_partner, row_partner


def step_along_z(group, half):
    return (group + 1) if half == 0 else (7 - group) * (1 - (group + 1) // 4)


def peer_at(z, y, core, dz, r, sign):
    return ((z + sign * dz + Z) % Z) * PLANE + ((y + sign * (r // 2) + Y) % Y) * CORES + (core + r % 2) % CORES


def wait_for(ref, sem):
    pltpu.make_async_copy(ref, ref, sem).wait()


def routed_kernel(
    slots, w_gate, w_up, w_down, ret,
    gate_v, up_v, down_v, recv, xrecv, rows_v, act_v, kept, xsend, xret, fin,
    d_send, d_recv, x_send, x_recv, b_send, b_recv, r_send, r_recv, w_send, w_recv, l_sem,
):
    sp, tp, z, y, core, weight_partner, row_partner = position()
    barrier = pltpu.get_barrier_semaphore()

    def greet(i, _):
        other = lax.rem(sp + i, Z * PLANE)
        pl.semaphore_signal(barrier, inc=1, device_id=(other, tp), device_id_type=MESH)
        return 0

    lax.fori_loop(1, Z * PLANE, greet, 0)
    for partner in (weight_partner, row_partner):
        pl.semaphore_signal(barrier, inc=1, device_id=(sp, partner), device_id_type=MESH)
    width = w_down.shape[2]
    half_units = w_down.shape[1]
    loads = [
        pltpu.make_async_copy(w_gate.at[0], gate_v.at[0], l_sem.at[0]),
        pltpu.make_async_copy(w_up.at[0], up_v.at[0], l_sem.at[1]),
        pltpu.make_async_copy(w_down.at[0], down_v.at[0:half_units], l_sem.at[2]),
    ]
    for load in loads:
        load.start()
    pltpu.make_async_copy(slots.at[sp], recv.at[SELF], d_recv.at[SELF]).start()
    pl.semaphore_wait(barrier, Z * PLANE + 1)

    def swap(i, src, dst):
        return pltpu.make_async_remote_copy(
            src_ref=src, dst_ref=dst, send_sem=w_send.at[i], recv_sem=w_recv.at[i],
            device_id=(sp, weight_partner), device_id_type=MESH,
        )

    swaps = [
        swap(0, w_gate.at[0], gate_v.at[1]),
        swap(1, w_up.at[0], up_v.at[1]),
        swap(2, w_down.at[0], down_v.at[half_units : 2 * half_units]),
    ]
    for group in range(GROUPS):
        for half in range(2):
            dz = step_along_z(group, half)
            base = group * PEERS + half * PLANE

            def send(r, _, dz=dz, base=base):
                other = peer_at(z, y, core, dz, r, 1)
                pltpu.make_async_remote_copy(
                    src_ref=slots.at[other], dst_ref=recv.at[base + r],
                    send_sem=d_send.at[base + r], recv_sem=d_recv.at[base + r],
                    device_id=(other, tp), device_id_type=MESH,
                ).start()
                return 0

            lax.fori_loop(1 if base == SELF else 0, PLANE, send, 0)
    for s in swaps:
        s.start()

    def cross(c, src, dst, send_sem, recv_sem):
        return pltpu.make_async_remote_copy(
            src_ref=src.at[pl.ds(c * PEERS, PEERS)], dst_ref=dst.at[pl.ds(c * PEERS, PEERS)],
            send_sem=send_sem.at[c], recv_sem=recv_sem.at[c],
            device_id=(sp, row_partner), device_id_type=MESH,
        )

    count = PEERS * CAP

    def stage(step, _):
        @pl.when(step < GROUPS)
        def arrive():
            def one(r, _):
                wait_for(recv.at[step * PEERS + r], d_recv.at[step * PEERS + r])
                return 0

            lax.fori_loop(0, PEERS, one, 0)
            cross(step, recv, xrecv, x_send, x_recv).start()

        @pl.when(step == 1)
        def weights():
            for load in loads:
                load.wait()
            for s in swaps:
                s.wait()

        @pl.when((step >= 1) & (step <= GROUPS))
        def compute():
            c = step - 1
            cross(c, recv, xrecv, x_send, x_recv).wait_recv()
            at = pl.ds(c * PEERS, PEERS)
            rows_v[0:count] = recv[at].astype(jnp.float32).reshape(count, width).astype(jnp.bfloat16)
            rows_v[count : 2 * count] = xrecv[at].astype(jnp.float32).reshape(count, width).astype(jnp.bfloat16)

            def activate(j, _):
                half, col = j // 2, pl.multiple_of((j % 2) * TILE, TILE)
                g = jnp.dot(rows_v[...], gate_v[half, :, pl.ds(col, TILE)], preferred_element_type=jnp.float32)
                u = jnp.dot(rows_v[...], up_v[half, :, pl.ds(col, TILE)], preferred_element_type=jnp.float32)
                g = jnp.minimum(g, LIMIT)
                u = jnp.clip(u, -LIMIT, LIMIT)
                act = (u + 1.0) * g * jax.nn.sigmoid(SLOPE * g)
                act_v[:, pl.ds(pl.multiple_of(j * TILE, TILE), TILE)] = act.astype(jnp.bfloat16)
                return 0

            lax.fori_loop(0, 2 * half_units // TILE, activate, 0)

            def project(n, _):
                cols = pl.ds(pl.multiple_of(n * TILE, TILE), TILE)
                out = jnp.dot(act_v[...], down_v[:, cols], preferred_element_type=jnp.float32)
                kept[c % 2, :, cols] = out[0:count]
                xsend[at, :, cols] = out[count : 2 * count].reshape(PEERS, CAP, TILE).astype(jnp.bfloat16)
                return 0

            lax.fori_loop(0, width // TILE, project, 0)
            cross(c, xsend, xret, b_send, b_recv).start()

        @pl.when(step >= 2)
        def give_back():
            c = step - 2
            cross(c, xsend, xret, b_send, b_recv).wait_recv()
            at = pl.ds(c * PEERS, PEERS)
            total = kept[c % 2].reshape(PEERS, CAP, width) + xret[at].astype(jnp.float32)
            fin[at] = total.astype(jnp.bfloat16)
            for half in range(2):
                dz = step_along_z(c, half)

                def send(r, _, dz=dz, half=half):
                    k = c * PEERS + half * PLANE + r
                    other = peer_at(z, y, core, dz, r, -1)

                    @pl.when(k != SELF)
                    def away():
                        pltpu.make_async_remote_copy(
                            src_ref=fin.at[k], dst_ref=ret.at[sp],
                            send_sem=r_send.at[k], recv_sem=r_recv.at[k],
                            device_id=(other, tp), device_id_type=MESH,
                        ).start()

                    @pl.when(k == SELF)
                    def here():
                        pltpu.make_async_copy(fin.at[k], ret.at[sp], r_recv.at[k]).start()

                    return 0

                lax.fori_loop(0, PLANE, send, 0)

        return 0

    lax.fori_loop(0, GROUPS + 2, stage, 0)

    def finish(k, _):
        wait_for(ret.at[k], r_recv.at[k])

        @pl.when(k != SELF)
        def away():
            wait_for(recv.at[k], d_send.at[k])
            wait_for(fin.at[k], r_send.at[k])

        return 0

    lax.fori_loop(0, Z * PLANE, finish, 0)
    for c in range(GROUPS):
        cross(c, recv, xrecv, x_send, x_recv).wait_send()
        cross(c, xsend, xret, b_send, b_recv).wait_send()


def routed(slots, w_gate, w_up, w_down):
    experts, cap, width = slots.shape
    units = w_down.shape[1]
    count = PEERS * CAP
    dma = pltpu.SemaphoreType.DMA
    vmem, hbm = pl.BlockSpec(memory_space=pltpu.VMEM), pl.BlockSpec(memory_space=pl.ANY)
    moved = pltpu.VMEM(slots.shape, jnp.bfloat16)
    return pl.pallas_call(
        routed_kernel,
        out_shape=jax.ShapeDtypeStruct(slots.shape, jnp.bfloat16),
        in_specs=[vmem, hbm, hbm, hbm],
        out_specs=vmem,
        scratch_shapes=[
            pltpu.VMEM((2, width, units), jnp.bfloat16),
            pltpu.VMEM((2, width, units), jnp.bfloat16),
            pltpu.VMEM((2 * units, width), jnp.bfloat16),
            moved,
            moved,
            pltpu.VMEM((2 * count, width), jnp.bfloat16),
            pltpu.VMEM((2 * count, 2 * units), jnp.bfloat16),
            pltpu.VMEM((2, count, width), jnp.float32),
            moved,
            moved,
            moved,
            dma((experts,)), dma((experts,)),
            dma((GROUPS,)), dma((GROUPS,)),
            dma((GROUPS,)), dma((GROUPS,)),
            dma((experts,)), dma((experts,)),
            dma((3,)), dma((3,)), dma((3,)),
        ],
        compiler_params=pltpu.CompilerParams(
            collective_id=0, has_side_effects=True, vmem_limit_bytes=56 * 2**20
        ),
        name="routed",
    )(slots, w_gate, w_up, w_down)


def slot_positions(route_ids, capacity):
    flat = route_ids.reshape(-1)
    order = jnp.arange(flat.shape[0], dtype=jnp.int32)
    earlier = (flat[:, None] == flat[None, :]) & (order[None, :] < order[:, None])
    rank = jnp.sum(earlier.astype(jnp.int32), axis=1)
    return (flat * capacity + rank).reshape(route_ids.shape)


def shards(
    glu_value,
    glu_gate,
    conv_kernel,
    norm_gain,
    mix_weight,
    residual,
    resid_gain,
    expert_ids,
    route_weight,
    w_gate,
    w_up,
    w_down,
    out_gain,
):
    gated_in = (
        glu_value.astype(jnp.float32) * jax.nn.sigmoid(glu_gate.astype(jnp.float32))
    ).astype(jnp.bfloat16)
    reach_back = conv_kernel.shape[0] - 1
    length = gated_in.shape[0]
    before_rows = shifted(gated_in[length - reach_back :], "sp", 1)
    extended = jnp.concatenate([before_rows, gated_in], axis=0).astype(jnp.float32)
    convolved = jnp.zeros(gated_in.shape, jnp.float32)
    for offset in range(reach_back + 1):
        convolved = convolved + conv_kernel[offset] * extended[offset : offset + length]
    channel_sum, squares = together(
        (jnp.sum(convolved, axis=1), jnp.sum(convolved * convolved, axis=1)), "tp"
    )
    centre = channel_sum / DC
    spread = squares / DC - centre * centre
    normed = (convolved - centre[:, None]) * lax.rsqrt(spread[:, None] + EPSILON) * norm_gain
    mix_in = jax.nn.silu(normed).astype(jnp.bfloat16)
    tp_count = lax.axis_size("tp")
    own_count = length // tp_count
    section = mix_in
    mixed_rows = sum_at_owner(
        jnp.dot(section, mix_weight, preferred_element_type=jnp.float32).astype(jnp.bfloat16),
        "tp",
        0,
    )
    hidden = normalize(residual.astype(jnp.float32) + mixed_rows, resid_gain).astype(jnp.bfloat16)
    experts = lax.axis_size("sp")
    width = hidden.shape[1]
    positions = slot_positions(expert_ids, CAP)
    places = jnp.arange(experts * CAP, dtype=jnp.int32)
    named = positions[:, :, None] == places
    held = jnp.any(named, axis=1).astype(jnp.bfloat16)
    slots = lax.dot_general(held, hidden, (((0,), (0,)), ((), ())), preferred_element_type=jnp.float32)
    slots = slots.astype(jnp.bfloat16).reshape(experts, CAP, width)
    returned = routed(slots, w_gate, w_up, w_down).reshape(experts * CAP, width)
    share = jnp.sum(jnp.where(named, route_weight[:, :, None], 0.0), axis=1)
    share_high = share.astype(jnp.bfloat16)
    share_low = (share - share_high.astype(jnp.float32)).astype(jnp.bfloat16)
    routed_sum = jnp.dot(share_high, returned, preferred_element_type=jnp.float32) + jnp.dot(
        share_low, returned, preferred_element_type=jnp.float32
    )
    return normalize(hidden.astype(jnp.float32) + routed_sum, out_gain).astype(jnp.bfloat16)


def solution(mesh):
    in_specs = (
        P("sp", "tp"),
        P("sp", "tp"),
        P(None, "tp"),
        P("tp"),
        P("tp", None),
        P(("sp", "tp"), None),
        P(),
        P(("sp", "tp"), None),
        P(("sp", "tp"), None),
        P("sp", None, "tp"),
        P("sp", None, "tp"),
        P("sp", "tp", None),
        P(),
    )
    out_specs = P(("sp", "tp"), None)
    return jax.shard_map(shards, mesh=mesh, in_specs=in_specs, out_specs=out_specs, check_vma=False)
```

time: 401 us -> 231 us (0.58)
  waiting for transfers between devices: 238 us -> 25.4 us
  Pallas kernels: 0 us -> 166 us
  blocking collectives: 70.1 us -> 8.03 us
  matrix products: 27.4 us -> 7.6 us
  between operations: 13.7 us -> 0.23 us
  local copies, waits for them, and re-layouts: 15.9 us -> 2.87 us
  starting transfers between devices: 20.5 us -> 9.15 us
    pallas_call x0 -> x1, Pallas kernels: none -> 166 us  [routed(): pl.pallas_call(routed_kernel, out_shape=jax.ShapeDtypeStruct(slots.shape,...]
    reduce_scatter x1 -> x0, waiting for transfers between devices: 84.3 us -> none  [shards(): lax.psum_scatter(jnp.dot(section, down_local, preferred_element_type=jnp....]
    all_gather x1 -> x0, waiting for transfers between devices: 81.1 us -> none  [work_in_pieces(): done.append(jax.vmap(apply)(lax.all_gather(section, axis), starts))]
    all_to_all x1 -> x0, blocking collectives: 62.1 us -> none  [shards(): lax.all_to_all(dispatched, 'sp', split_axis=0, concat_axis=0, tiled=True)]
    all_to_all x1 -> x0, waiting for transfers between devices: 49.4 us -> none  [shards(): lax.all_to_all(expert_out, 'sp', split_axis=0, concat_axis=0, tiled=True)]
    dot_general x4 -> x3, matrix products: 22.6 us -> 4.84 us  [the longest x1 2.18 us: shards(): jnp.dot(share_high, returned, preferred_element_type=jnp.float32)]
    all_to_all x1 -> x0, starting transfers between devices: 11.1 us -> none  [shards(): lax.all_to_all(expert_out, 'sp', split_axis=0, concat_axis=0, tiled=True)]
    gather x2 -> x0, local copies, waits for them, and re-layouts: 8.55 us -> none  [the longest x1 5.21 us: shards(): returned_rows.reshape(experts * capacity, width)[positions.reshape(-1)]]
  transfers between devices with their start and end apart: 5 -> 2, of which waited for: 4 -> 1; matrix products, arithmetic and copies ran while one was open for 1% -> 1% of each run, Pallas kernels for 0% -> 0%
where the time goes in v2:
time: 231 us
  Pallas kernels  166 us (72%)
  waiting for transfers between devices  25.4 us (11%)
  other arithmetic  11.5 us (5%)
  starting transfers between devices  9.15 us (4%)
  blocking collectives  8.03 us (3%)
  matrix products  7.6 us (3%)
  local copies, waits for them, and re-layouts  2.87 us (1%)
    pallas_call x1, Pallas kernels, routed(): pl.pallas_call(routed_kernel, out_shape=jax.ShapeDtypeStruct(slots.shape,...  166 us
    all_to_all x1, waiting for transfers between devices, sum_at_owner(): lax.all_to_all(tiles, axis, split_axis=0, concat_axis=0, tiled=True)  25.4 us
    all_to_all x1, blocking collectives, copy_for_each(): lax.all_to_all(jnp.broadcast_to(array[None], (count, *array.shape)), axis...  8.03 us
    reduce_sum x1, other arithmetic, shards(): jnp.sum(convolved, axis=1)  5.04 us
  transfers between devices with their start and end apart: 2, of which 1 were waited for; matrix products, arithmetic and copies ran while one was open for 1% of the time, Pallas kernels for 0%

profile of v2, /device:TPU:1, one launch (start us, length us, event | category | flops | bytes accessed | tf_op | source)
XLA Modules:
  0.0 230.8 jit_solution(256824705573225663)
XLA Ops:
  0.0 0.0 copy-start
  0.0 1.6 multiply_convert_fusion.3
  1.7 4.6 %collective-permute-start = (bf16[30,512]{1,0:T(8,128)(2,1)S(1)}, bf16[30,512]{1,0:T(8,128)(2,1)S(1)}, u32[]{:S(2)}, u32[]{:S(2)}) collective-permute-start(bf16[30,512]{1,0:T(8,128)(2,1)S(1)} %slice.260), channel_id=1, source_target_pairs={{0,4},{4,8},{8,12},{12,16},{16,20},{20,24},{24,28},{28,32},{32,36}... | collective-permute-start | bytes 92168 | tf_op jit(solution)/shard_map/ppermute | solution.py:19
  6.3 1.2 fusion.47
  7.4 1.0 fusion.48
  8.4 0.0 collective-permute-done
  8.5 0.2 maximum_convert_fusion
  8.6 0.0 copy-start.7
  8.6 5.0 %fusion.45 = (f32[512]{0:T(512)S(1)}, f32[512]{0:T(512)S(1)}, f32[512,512]{1,0:T(8,128)S(1)}) fusion(f32[542,512]{1,0:T(8,128)S(1)} %maximum_convert_fusion, f32[512]{0:T(512)S(1)} %bitcast.74, f32[512]{0:T(512)S(1)} %bitcast.75, f32[512]{0:T(512)S(1)} %bitcast.46, f32[512]{0:T(512)S(1)} %bitcast.47, f32[512]{0:T(512)S(1)} %bitcast.48, f32[512]{0:T(512)S(1)} %bitcast.49, ...), kind=kLoop, calls=%fused_computation.102 | loop fusion | flops 16776192 | bytes 33622016 | tf_op jit(solution)/shard_map/reduce_sum | solution.py:329
  13.7 8.0 %all_to_all.11 = f32[4,1,1024]{2,1,0:T(1,128)S(1)} all-to-all(f32[4,1,1024]{2,1,0:T(1,128)S(1)} %broadcast_in_dim.10), channel_id=1, replica_groups=mesh['sp'=64,'tp'=4] {'tp'}, dimensions={0} | all-to-all | bytes 32768 | tf_op jit(solution)/shard_map/all_to_all | solution.py:24
  21.8 0.0 copy-done
  21.8 0.0 copy-done.7
  21.8 2.8 %convolution_convert_fusion.1 = bf16[512,2048]{1,0:T(8,128)(2,1)} fusion(bf16[512,2048]{1,0:T(8,128)(2,1)S(1)} %copy-done, f32[512,512]{1,0:T(8,128)S(1)} %get-tuple-element.7, f32[512]{0:T(512)S(1)} %copy-done.7, f32[512]{0:T(512)S(1)} %get-tuple-element.40, f32[512]{0:T(512)S(1)} %get-tuple-element.39), kind=kOutput, calls=%fused_computation.2 | convolution fusion | flops 1076887552 | bytes 5249024 | tf_op jit(solution)/shard_map/dot_general | solution.py:339
  24.6 0.0 copy-start.5
  24.6 0.0 copy-start.6
  24.6 4.6 %all-to-all-start.1 = ((bf16[4,128,2048]{2,1,0:T(8,128)(2,1)}), bf16[4,128,2048]{2,1,0:T(8,128)(2,1)}, u32[]{:S(2)}, u32[]{:S(2)}) async-start(bf16[4,128,2048]{2,1,0:T(8,128)(2,1)} %bitcast.44), calls=%async_computation.1 | async-start | bytes 4194304 | tf_op jit(solution)/shard_map/all_to_all | solution.py:48
  29.2 0.0 copy-done.5
  29.2 0.0 copy-start.2
  29.2 0.1 copy.30
  29.3 0.1 eq.28
  29.4 0.2 convert_reduce_fusion.1
  29.6 0.1 reduce_sum.99
  29.8 0.1 copy.31
  29.8 0.1 fusion.35
  30.0 0.0 copy-done.6
  30.0 0.1 select_reduce_fusion
  30.1 25.4 %all-to-all-done.1 = bf16[4,128,2048]{2,1,0:T(8,128)(2,1)} async-done(((bf16[4,128,2048]{2,1,0:T(8,128)(2,1)}), bf16[4,128,2048]{2,1,0:T(8,128)(2,1)}, u32[]{:S(2)}, u32[]{:S(2)}) %all-to-all-start.1) | async-done | bytes 2097184 | tf_op jit(solution)/shard_map/all_to_all | solution.py:48
  55.6 2.1 convert_reduce_fusion
  57.7 0.0 copy-done.2
  57.7 0.0 copy-start.3
  57.7 0.2 fusion.40
  57.9 0.3 multiply_reduce_fusion.1
  58.2 0.2 copy-done.3
  58.4 0.3 multiply_convert_fusion.1
  58.7 2.1 fusion.slots
  60.8 165.9 %routed.1 = bf16[64,8,2048]{2,1,0:T(8,128)(2,1)} custom-call(bf16[64,8,2048]{2,1,0:T(8,128)(2,1)} %fusion.slots, bf16[1,2048,512]{2,1,0:T(8,128)(2,1)} %w_gate.1, bf16[1,2048,512]{2,1,0:T(8,128)(2,1)} %w_up.1, bf16[1,512,2048]{2,1,0:T(8,128)(2,1)} %w_down.1), custom_call_target="tpu_custom_call" | custom-call | tf_op jit(solution)/shard_map/routed/pallas_call | solution.py:265
  226.7 0.0 copy-start.1
  226.7 2.2 fusion.3
  228.9 0.0 copy-done.1
  228.9 0.0 copy-start.4
  228.9 0.6 fusion.49
  229.5 0.3 multiply_reduce_fusion
  229.8 0.0 copy-done.4
  229.8 1.0 multiply_convert_fusion
  (10 shorter events, 0.1 us)
Async XLA Ops:
  0.0 21.8 %copy-start = (bf16[512,2048]{1,0:T(8,128)(2,1)S(1)}, bf16[512,2048]{1,0:T(8,128)(2,1)}, u32[]{:S(2)}) copy-start(bf16[512,2048]{1,0:T(8,128)(2,1)} %param.17) | copy-start | bytes 6291460
  1.7 6.8 %collective-permute-start = (bf16[30,512]{1,0:T(8,128)(2,1)S(1)}, bf16[30,512]{1,0:T(8,128)(2,1)S(1)}, u32[]{:S(2)}, u32[]{:S(2)}) collective-permute-start(bf16[30,512]{1,0:T(8,128)(2,1)S(1)} %slice.260), channel_id=1, source_target_pairs={{0,4},{4,8},{8,12},{12,16},{16,20},{20,24},{24,28},{28,32},{32,36}... | collective-permute-start | bytes 92168 | tf_op jit(solution)/shard_map/ppermute | solution.py:19
  8.6 13.2 %copy-start.7 = (f32[512]{0:T(512)S(1)}, f32[512]{0:T(512)}, u32[]{:S(2)}) copy-start(f32[512]{0:T(512)} %param.16) | copy-start | bytes 6148
  24.6 4.6 %copy-start.5 = (s32[128,2]{0,1:T(2,128)S(1)}, s32[128,2]{0,1:T(2,128)}, u32[]{:S(2)}) copy-start(s32[128,2]{0,1:T(2,128)} %param.20) | copy-start | bytes 3076
  24.6 5.4 %copy-start.6 = (f32[128,2]{0,1:T(2,128)S(1)}, f32[128,2]{0,1:T(2,128)}, u32[]{:S(2)}) copy-start(f32[128,2]{0,1:T(2,128)} %param.21) | copy-start | bytes 3076
  24.6 31.0 %all-to-all-start.1 = ((bf16[4,128,2048]{2,1,0:T(8,128)(2,1)}), bf16[4,128,2048]{2,1,0:T(8,128)(2,1)}, u32[]{:S(2)}, u32[]{:S(2)}) async-start(bf16[4,128,2048]{2,1,0:T(8,128)(2,1)} %bitcast.44), calls=%async_computation.1 | async-start | bytes 4194304 | tf_op jit(solution)/shard_map/all_to_all | solution.py:48
  29.2 28.5 %copy-start.2 = (bf16[128,2048]{1,0:T(8,128)(2,1)S(1)}, bf16[128,2048]{1,0:T(8,128)(2,1)}, u32[]{:S(2)}) copy-start(bf16[128,2048]{1,0:T(8,128)(2,1)} %param.18) | copy-start | bytes 1572868
  57.7 0.7 copy-start.3
  226.7 2.2 copy-start.1
  228.9 0.8 copy-start.4

commit v3 on v2

v3 whole, which is shorter than its diff:
```python
import jax
import jax.numpy as jnp
from jax import lax
from jax.experimental import pallas as pl
from jax.experimental.pallas import tpu as pltpu
from jax.sharding import PartitionSpec as P

DC = 2048
EPSILON = 1e-05
LIMIT = 7.0
SLOPE = 1.702
Z, Y, CORES, N_TP = 8, 4, 2, 4
PLANE = Y * CORES
N_SP = Z * PLANE
GROUPS = 4
PEERS = 2 * PLANE
SELF_GROUP = 3
SELF = SELF_GROUP * PEERS + PLANE
CAP = 8
TILE = 256
LANES = 128
TAPS = 31
HALO = 32
ROWS = 512
BLOCK = 128
STRIPE = 64
MESH = pl.DeviceIdType.MESH
F32, BF16 = jnp.float32, jnp.bfloat16


def normalize(values, gain_vector):
    centre = jnp.mean(values, axis=-1, keepdims=True)
    spread = jnp.mean(jnp.square(values - centre), axis=-1, keepdims=True)
    return (values - centre) * lax.rsqrt(spread + EPSILON) * gain_vector


def position():
    sp, tp = lax.axis_index("sp"), lax.axis_index("tp")
    z, y, core = sp // PLANE, (sp // CORES) % Y, sp % CORES
    near, far = tp + 1 - 2 * (tp % 2), 3 - tp
    weight_partner = near * (1 - core) + far * core
    row_partner = near * core + far * (1 - core)
    return sp, tp, z, y, core, weight_partner, row_partner


def step_along_z(group, half):
    return (group + 1) if half == 0 else (7 - group) * (1 - (group + 1) // 4)


def peer_at(z, y, core, dz, r, sign):
    return ((z + sign * dz + Z) % Z) * PLANE + ((y + sign * (r // 2) + Y) % Y) * CORES + (core + r % 2) % CORES


def wait_for(ref, sem):
    pltpu.make_async_copy(ref, ref, sem).wait()


def layer_kernel(
    value, gate, taps, norm_gain, residual, resid_gain, out_gain, ids, weights,
    mix_weight, w_gate, w_up, w_down,
    out,
    ext, halo_send, halo_recv, conv_v, stat_cols, stat_rows, stats_send, stats_recv, mix_in, mix_v,
    a_send_v, a_recv_v, b_send_v, b_recv_v, acc, hidden, held, share, slots, ret,
    gate_v, up_v, down_v, recv, xrecv, rows_v, act_v, kept, xsend, xret, fin,
    d_send, d_recv, x_send, x_recv, b_send, b_recv, r_send, r_recv, w_send, w_recv, l_sem,
    h_sem, s_send, s_recv, ra_send, ra_recv, rb_send, rb_recv,
):
    sp, tp, z, y, core, weight_partner, row_partner = position()
    barrier = pltpu.get_barrier_semaphore()

    def greet(i, _):
        other = lax.rem(sp + i, N_SP)
        pl.semaphore_signal(barrier, inc=1, device_id=(other, tp), device_id_type=MESH)
        return 0

    lax.fori_loop(1, N_SP, greet, 0)
    for i in range(1, N_TP):
        pl.semaphore_signal(barrier, inc=1, device_id=(sp, (tp + i) % N_TP), device_id_type=MESH)
    width = w_down.shape[2]
    half_units = w_down.shape[1]
    channels = value.shape[1]
    loads = [
        pltpu.make_async_copy(mix_weight, mix_v, l_sem.at[3]),
        pltpu.make_async_copy(w_gate.at[0], gate_v.at[0], l_sem.at[0]),
        pltpu.make_async_copy(w_up.at[0], up_v.at[0], l_sem.at[1]),
        pltpu.make_async_copy(w_down.at[0], down_v.at[0:half_units], l_sem.at[2]),
    ]
    for load in loads:
        load.start()

    lane_groups = channels // LANES

    def gated(rows, cols):
        product = value[rows, cols].astype(F32) * jax.nn.sigmoid(gate[rows, cols].astype(F32))
        return product.astype(BF16)

    for g in range(lane_groups):
        halo_send[g] = gated(pl.ds(ROWS - HALO, HALO), pl.ds(g * LANES, LANES))

    def gate_rows(i, _):
        for g in range(lane_groups):
            at = pl.ds(pl.multiple_of(i * STRIPE, STRIPE), STRIPE)
            to = pl.ds(pl.multiple_of(i * STRIPE + HALO, HALO), STRIPE)
            ext[g, to] = gated(at, pl.ds(g * LANES, LANES)).astype(F32)
        return 0

    lax.fori_loop(0, ROWS // STRIPE, gate_rows, 0)
    pl.semaphore_wait(barrier, N_SP - 1 + N_TP - 1)
    halo_copy = pltpu.make_async_remote_copy(
        src_ref=halo_send, dst_ref=halo_recv, send_sem=h_sem.at[0], recv_sem=h_sem.at[1],
        device_id=(lax.rem(sp + 1, N_SP), tp), device_id_type=MESH,
    )
    halo_copy.start()

    def swap(i, src, dst):
        return pltpu.make_async_remote_copy(
            src_ref=src, dst_ref=dst, send_sem=w_send.at[i], recv_sem=w_recv.at[i],
            device_id=(sp, weight_partner), device_id_type=MESH,
        )

    def rows_of(ref, first, last):
        return ref.at[pl.ds(first, last - first)]

    cuts = (0, 512, 1024, 2048)
    swaps = [
        swap(i, w_gate.at[0, pl.ds(f, l - f)], gate_v.at[1, pl.ds(f, l - f)])
        for i, (f, l) in enumerate(zip(cuts, cuts[1:]))
    ] + [
        swap(3, w_up.at[0], up_v.at[1]),
        swap(4, w_down.at[0], down_v.at[half_units : 2 * half_units]),
    ]
    swaps[0].start()

    lane = lax.broadcasted_iota(jnp.int32, (STRIPE, LANES), 1)

    def convolve(i):
        first = pl.multiple_of(i * STRIPE, STRIPE)
        total, square = jnp.zeros((STRIPE, LANES), F32), jnp.zeros((STRIPE, LANES), F32)
        for g in range(lane_groups):
            sums = jnp.zeros((STRIPE, LANES), F32)
            for k in range(TAPS):
                tap = taps[k : k + 1, g * LANES : (g + 1) * LANES]
                sums = sums + tap * ext[g, pl.ds(first + (HALO - TAPS + 1 + k), STRIPE)]
            conv_v[g, pl.ds(first, STRIPE)] = sums
            total, square = total + sums, square + sums * sums
        total = jnp.sum(total, axis=1, keepdims=True)
        square = jnp.sum(square, axis=1, keepdims=True)
        stat_cols[pl.ds(first, STRIPE)] = jnp.where(lane == 0, total, jnp.where(lane == 1, square, 0.0))

    def convolve_step(i, _):
        convolve(i)
        return 0

    lax.fori_loop(1, ROWS // STRIPE, convolve_step, 0)
    halo_copy.wait_recv()
    for g in range(lane_groups):
        ext[g, 0:HALO] = jnp.where(sp > 0, halo_recv[g].astype(F32), 0.0)
    convolve(0)
    for i in range(ROWS // LANES):
        at = slice(i * LANES, (i + 1) * LANES)
        stats_send[:, at] = jnp.transpose(stat_cols[at, :])[0:8]
    stat_copies = [
        pltpu.make_async_remote_copy(
            src_ref=stats_send, dst_ref=stats_recv.at[j - 1], send_sem=s_send.at[j - 1], recv_sem=s_recv.at[j - 1],
            device_id=(sp, (tp + j) % N_TP), device_id_type=MESH,
        )
        for j in (2, 1, 3)
    ]
    for c in stat_copies:
        c.start()
    swaps[1].start()

    experts = N_SP
    spot = lax.broadcasted_iota(jnp.int32, (experts, BLOCK), 0)
    one = [(spot == ids[j : j + 1, :]).astype(BF16) for j in range(2)]
    before = lax.broadcasted_iota(jnp.int32, (BLOCK, BLOCK), 0) < lax.broadcasted_iota(jnp.int32, (BLOCK, BLOCK), 1)
    earlier = jnp.dot(one[0] + one[1], before.astype(BF16), preferred_element_type=F32)
    owner = lax.broadcasted_iota(jnp.int32, (experts * CAP, experts), 0) // CAP
    spread_out = (owner == lax.broadcasted_iota(jnp.int32, (experts * CAP, experts), 1)).astype(BF16)
    rank = jnp.dot(spread_out, earlier.astype(BF16), preferred_element_type=F32)
    in_rank = rank == (lax.broadcasted_iota(jnp.int32, (experts * CAP, BLOCK), 0) % CAP).astype(F32)
    hits = [
        jnp.where(in_rank, jnp.dot(spread_out, o, preferred_element_type=F32), 0.0) for o in one
    ]
    held[...] = (hits[0] + hits[1]).astype(BF16)
    shares = hits[0] * weights[0:1, :] + hits[1] * weights[1:2, :]
    for i in range(experts * CAP // LANES):
        at = slice(i * LANES, (i + 1) * LANES)
        part = jnp.transpose(shares[at, :])
        high = part.astype(BF16)
        share[0:BLOCK, at] = high
        share[BLOCK : 2 * BLOCK, at] = (part - high.astype(F32)).astype(BF16)
    stat_rows[...] = jnp.zeros_like(stat_rows)

    for c in stat_copies:
        c.wait_recv()
    sums = stats_send[...] + stats_recv[0] + stats_recv[1] + stats_recv[2]
    centre = sums[0:1] / DC
    scale = lax.rsqrt(sums[1:2] / DC - centre * centre + EPSILON)
    stat_rows[0:1] = centre
    stat_rows[1:2] = scale

    loads[0].wait()

    def mix_rows(b):
        at = pl.ds(pl.multiple_of(b * BLOCK, BLOCK), BLOCK)
        columns = jnp.transpose(stat_rows[:, at])
        for g in range(lane_groups):
            lanes = slice(g * LANES, (g + 1) * LANES)
            v = (conv_v[g, at] - columns[:, 0:1]) * columns[:, 1:2] * norm_gain[:, lanes]
            mix_in[at, lanes] = (v / (1.0 + jnp.exp(-v))).astype(BF16)

    half_width = width // 2

    def project_rows(b, half, into):
        at = pl.ds(pl.multiple_of(b * BLOCK, BLOCK), BLOCK)

        def one_tile(n, _):
            col = pl.multiple_of(n * TILE, TILE)
            cols = pl.ds(pl.multiple_of(half * half_width + n * TILE, TILE), TILE)
            into(pl.ds(col, TILE), jnp.dot(mix_in[at, :], mix_v[:, cols], preferred_element_type=F32))
            return 0

        lax.fori_loop(0, half_width // TILE, one_tile, 0)

    def to_neighbour(src, dst, send_sem, recv_sem, side):
        return pltpu.make_async_remote_copy(
            src_ref=src, dst_ref=dst, send_sem=send_sem, recv_sem=recv_sem,
            device_id=(sp, (tp + (1 if side == 0 else N_TP - 1)) % N_TP), device_id_type=MESH,
        )

    far_copies = [
        to_neighbour(a_send_v.at[i], a_recv_v.at[i], ra_send.at[i], ra_recv.at[i], i) for i in range(2)
    ]
    near_copies = [
        [
            to_neighbour(
                b_send_v.at[i, h], b_recv_v.at[i, h], rb_send.at[2 * i + h], rb_recv.at[2 * i + h], i
            )
            for h in range(2)
        ]
        for i in range(2)
    ]
    far = (tp + 2) % N_TP
    sides = [(tp + 1) % N_TP, (tp + N_TP - 1) % N_TP]
    mix_rows(far)
    for i in range(2):

        def keep(cols, product, i=i):
            a_send_v[i, :, cols] = product.astype(BF16)

        project_rows(far, i, keep)
        far_copies[i].start()
    for i in range(2):
        mix_rows(sides[i])

        def keep(cols, product, i=i):
            b_send_v[i, 1 - i, :, cols] = product.astype(BF16)

        project_rows(sides[i], 1 - i, keep)
        near_copies[i][1 - i].start()
    for i in range(2):
        far_copies[i].wait_recv()

        def keep(cols, product, i=i):
            b_send_v[i, i, :, cols] = (product + a_recv_v[i, :, cols].astype(F32)).astype(BF16)

        project_rows(sides[i], i, keep)
        near_copies[i][i].start()
    for s in swaps[2:]:
        s.start()
    mix_rows(tp)
    for h in range(2):

        def keep(cols, product, h=h):
            acc[h, :, cols] = product

        project_rows(tp, h, keep)
    for i in range(2):
        near_copies[i][1 - i].wait_recv()
    for i in range(2):
        near_copies[i][i].wait_recv()

    strip = 16

    def norm_rows(i, _):
        at = pl.ds(pl.multiple_of(i * strip, strip), strip)
        halves = [
            acc[h, at] + b_recv_v[0, h, at].astype(F32) + b_recv_v[1, h, at].astype(F32) for h in range(2)
        ]
        total = jnp.concatenate(halves, axis=1) + residual[at].astype(F32)
        hidden[at] = normalize(total, resid_gain[...]).astype(BF16)
        return 0

    lax.fori_loop(0, BLOCK // strip, norm_rows, 0)

    def fill_slots(n, _):
        cols = pl.ds(pl.multiple_of(n * TILE, TILE), TILE)
        picked = jnp.dot(held[...], hidden[:, cols], preferred_element_type=F32)
        slots[:, :, cols] = picked.reshape(experts, CAP, TILE).astype(BF16)
        return 0

    lax.fori_loop(0, width // TILE, fill_slots, 0)

    pltpu.make_async_copy(slots.at[sp], recv.at[SELF], d_recv.at[SELF]).start()
    for group in range(GROUPS):
        for half in range(2):
            dz = step_along_z(group, half)
            base = group * PEERS + half * PLANE

            def send(r, _, dz=dz, base=base):
                other = peer_at(z, y, core, dz, r, 1)
                pltpu.make_async_remote_copy(
                    src_ref=slots.at[other], dst_ref=recv.at[base + r],
                    send_sem=d_send.at[base + r], recv_sem=d_recv.at[base + r],
                    device_id=(other, tp), device_id_type=MESH,
                ).start()
                return 0

            lax.fori_loop(1 if base == SELF else 0, PLANE, send, 0)
    def cross(c, src, dst, send_sem, recv_sem):
        return pltpu.make_async_remote_copy(
            src_ref=src.at[pl.ds(c * PEERS, PEERS)], dst_ref=dst.at[pl.ds(c * PEERS, PEERS)],
            send_sem=send_sem.at[c], recv_sem=recv_sem.at[c],
            device_id=(sp, row_partner), device_id_type=MESH,
        )

    count = PEERS * CAP

    def stage(step, _):
        @pl.when(step < GROUPS)
        def arrive():
            def one(r, _):
                wait_for(recv.at[step * PEERS + r], d_recv.at[step * PEERS + r])
                return 0

            lax.fori_loop(0, PEERS, one, 0)
            cross(step, recv, xrecv, x_send, x_recv).start()

        @pl.when(step == 0)
        def gate_weights():
            for load in loads[1:]:
                load.wait()
            for s in swaps[:-1]:
                s.wait_recv()

        @pl.when((step >= 1) & (step <= GROUPS))
        def compute():
            c = step - 1
            cross(c, recv, xrecv, x_send, x_recv).wait_recv()
            at = pl.ds(c * PEERS, PEERS)
            rows_v[0:count] = recv[at].astype(jnp.float32).reshape(count, width).astype(jnp.bfloat16)
            rows_v[count : 2 * count] = xrecv[at].astype(jnp.float32).reshape(count, width).astype(jnp.bfloat16)

            def activate(j, _):
                half, col = j // 2, pl.multiple_of((j % 2) * TILE, TILE)
                g = jnp.dot(rows_v[...], gate_v[half, :, pl.ds(col, TILE)], preferred_element_type=jnp.float32)
                u = jnp.dot(rows_v[...], up_v[half, :, pl.ds(col, TILE)], preferred_element_type=jnp.float32)
                g = jnp.minimum(g, LIMIT)
                u = jnp.clip(u, -LIMIT, LIMIT)
                act = (u + 1.0) * g * jax.nn.sigmoid(SLOPE * g)
                act_v[:, pl.ds(pl.multiple_of(j * TILE, TILE), TILE)] = act.astype(jnp.bfloat16)
                return 0

            lax.fori_loop(0, 2 * half_units // TILE, activate, 0)

            @pl.when(step == 1)
            def down_weights():
                swaps[-1].wait_recv()


            def project(n, _):
                cols = pl.ds(pl.multiple_of(n * TILE, TILE), TILE)
                out = jnp.dot(act_v[...], down_v[:, cols], preferred_element_type=jnp.float32)
                kept[c % 2, :, cols] = out[0:count]
                xsend[at, :, cols] = out[count : 2 * count].reshape(PEERS, CAP, TILE).astype(jnp.bfloat16)
                return 0

            lax.fori_loop(0, width // TILE, project, 0)
            cross(c, xsend, xret, b_send, b_recv).start()

        @pl.when(step >= 2)
        def give_back():
            c = step - 2
            cross(c, xsend, xret, b_send, b_recv).wait_recv()
            at = pl.ds(c * PEERS, PEERS)
            total = kept[c % 2].reshape(PEERS, CAP, width) + xret[at].astype(jnp.float32)
            fin[at] = total.astype(jnp.bfloat16)
            for half in range(2):
                dz = step_along_z(c, half)

                def send(r, _, dz=dz, half=half):
                    k = c * PEERS + half * PLANE + r
                    other = peer_at(z, y, core, dz, r, -1)

                    @pl.when(k != SELF)
                    def away():
                        pltpu.make_async_remote_copy(
                            src_ref=fin.at[k], dst_ref=ret.at[sp],
                            send_sem=r_send.at[k], recv_sem=r_recv.at[k],
                            device_id=(other, tp), device_id_type=MESH,
                        ).start()

                    @pl.when(k == SELF)
                    def here():
                        pltpu.make_async_copy(fin.at[k], ret.at[sp], r_recv.at[k]).start()

                    return 0

                lax.fori_loop(0, PLANE, send, 0)

        return 0

    lax.fori_loop(0, GROUPS + 2, stage, 0)

    def finish(k, _):
        wait_for(ret.at[k], r_recv.at[k])

        @pl.when(k != SELF)
        def away():
            wait_for(recv.at[k], d_send.at[k])
            wait_for(fin.at[k], r_send.at[k])

        return 0

    lax.fori_loop(0, Z * PLANE, finish, 0)
    for c in range(GROUPS):
        cross(c, recv, xrecv, x_send, x_recv).wait_send()
        cross(c, xsend, xret, b_send, b_recv).wait_send()
    for copy in [halo_copy, *swaps, *stat_copies, *far_copies, *near_copies[0], *near_copies[1]]:
        copy.wait_send()

    def gather_rows(n, _):
        cols = pl.ds(pl.multiple_of(n * TILE, TILE), TILE)
        rows = ret[:, :, cols].astype(F32).reshape(experts * CAP, TILE).astype(BF16)
        both = jnp.dot(share[...], rows, preferred_element_type=F32)
        half = n // (half_width // TILE)
        to = pl.ds(pl.multiple_of(n * TILE - half * half_width, TILE), TILE)
        acc[half, :, to] = both[0:BLOCK] + both[BLOCK : 2 * BLOCK] + hidden[:, cols].astype(F32)
        return 0

    lax.fori_loop(0, width // TILE, gather_rows, 0)

    def last_norm(i, _):
        at = pl.ds(pl.multiple_of(i * strip, strip), strip)
        total = jnp.concatenate([acc[0, at], acc[1, at]], axis=1)
        out[at] = normalize(total, out_gain[...]).astype(BF16)
        return 0

    lax.fori_loop(0, BLOCK // strip, last_norm, 0)


def shards(
    glu_value,
    glu_gate,
    conv_kernel,
    norm_gain,
    mix_weight,
    residual,
    resid_gain,
    expert_ids,
    route_weight,
    w_gate,
    w_up,
    w_down,
    out_gain,
):
    width = residual.shape[1]
    units = w_down.shape[1]
    channels = glu_value.shape[1]
    groups = channels // LANES
    experts = N_SP
    count = PEERS * CAP
    dma = pltpu.SemaphoreType.DMA
    vmem, hbm = pl.BlockSpec(memory_space=pltpu.VMEM), pl.BlockSpec(memory_space=pl.ANY)
    moved = pltpu.VMEM((experts, CAP, width), BF16)
    return pl.pallas_call(
        layer_kernel,
        out_shape=jax.ShapeDtypeStruct((BLOCK, width), BF16),
        in_specs=[vmem] * 9 + [hbm] * 4,
        out_specs=vmem,
        scratch_shapes=[
            pltpu.VMEM((groups, ROWS + HALO, LANES), F32),
            pltpu.VMEM((groups, HALO, LANES), BF16),
            pltpu.VMEM((groups, HALO, LANES), BF16),
            pltpu.VMEM((groups, ROWS, LANES), F32),
            pltpu.VMEM((ROWS, LANES), F32),
            pltpu.VMEM((LANES, ROWS), F32),
            pltpu.VMEM((8, ROWS), F32),
            pltpu.VMEM((N_TP - 1, 8, ROWS), F32),
            pltpu.VMEM((ROWS, channels), BF16),
            pltpu.VMEM((channels, width), BF16),
            pltpu.VMEM((2, BLOCK, width // 2), BF16),
            pltpu.VMEM((2, BLOCK, width // 2), BF16),
            pltpu.VMEM((2, 2, BLOCK, width // 2), BF16),
            pltpu.VMEM((2, 2, BLOCK, width // 2), BF16),
            pltpu.VMEM((2, BLOCK, width // 2), F32),
            pltpu.VMEM((BLOCK, width), BF16),
            pltpu.VMEM((experts * CAP, BLOCK), BF16),
            pltpu.VMEM((2 * BLOCK, experts * CAP), BF16),
            moved,
            moved,
            pltpu.VMEM((2, width, units), BF16),
            pltpu.VMEM((2, width, units), BF16),
            pltpu.VMEM((2 * units, width), BF16),
            moved,
            moved,
            pltpu.VMEM((2 * count, width), BF16),
            pltpu.VMEM((2 * count, 2 * units), BF16),
            pltpu.VMEM((2, count, width), F32),
            moved,
            moved,
            moved,
            dma((experts,)), dma((experts,)),
            dma((GROUPS,)), dma((GROUPS,)),
            dma((GROUPS,)), dma((GROUPS,)),
            dma((experts,)), dma((experts,)),
            dma((5,)), dma((5,)), dma((4,)),
            dma((2,)), dma((3,)), dma((3,)),
            dma((2,)), dma((2,)), dma((4,)), dma((4,)),
        ],
        compiler_params=pltpu.CompilerParams(
            collective_id=0, has_side_effects=True, vmem_limit_bytes=60 * 2**20
        ),
        name="layer",
    )(
        glu_value, glu_gate, conv_kernel, norm_gain[None], residual, resid_gain[None], out_gain[None],
        expert_ids.T, route_weight.T, mix_weight, w_gate, w_up, w_down,
    )


def solution(mesh):
    in_specs = (
        P("sp", "tp"),
        P("sp", "tp"),
        P(None, "tp"),
        P("tp"),
        P("tp", None),
        P(("sp", "tp"), None),
        P(),
        P(("sp", "tp"), None),
        P(("sp", "tp"), None),
        P("sp", None, "tp"),
        P("sp", None, "tp"),
        P("sp", "tp", None),
        P(),
    )
    out_specs = P(("sp", "tp"), None)
    return jax.shard_map(shards, mesh=mesh, in_specs=in_specs, out_specs=out_specs, check_vma=False)
```

time: 231 us -> 188 us (0.81)
  waiting for transfers between devices: 25.4 us -> 0 us
  Pallas kernels: 166 us -> 185 us
  other arithmetic: 11.5 us -> 0 us
  starting transfers between devices: 9.15 us -> 0 us
  blocking collectives: 8.03 us -> 0 us
  matrix products: 7.6 us -> 0 us
    all_to_all x1 -> x0, waiting for transfers between devices: 25.4 us -> none  [sum_at_owner(): lax.all_to_all(tiles, axis, split_axis=0, concat_axis=0, tiled=True)]
    pallas_call x1, Pallas kernels: 166 us -> 185 us  [shards(): pl.pallas_call(layer_kernel, out_shape=jax.ShapeDtypeStruct((BLOCK, width...]
    reduce_sum x8 -> x0, other arithmetic: 8.25 us -> none  [the longest x1 5.04 us: shards(): jnp.sum(convolved, axis=1)]
    all_to_all x1 -> x0, blocking collectives: 8.03 us -> none  [copy_for_each(): lax.all_to_all(jnp.broadcast_to(array[None], (count, *array.shape)), axis...]
    dot_general x4 -> x0, matrix products: 7.6 us -> none  [the longest x1 2.76 us: shards(): jnp.dot(section, mix_weight, preferred_element_type=jnp.float32)]
    ppermute x1 -> x0, starting transfers between devices: 4.58 us -> none  [shifted(): return lax.ppermute(block, axis, route)]
    all_to_all x1 -> x0, starting transfers between devices: 4.57 us -> none  [sum_at_owner(): lax.all_to_all(tiles, axis, split_axis=0, concat_axis=0, tiled=True)]
    convert_element_type x4 -> x0, other arithmetic: 3.08 us -> none  [the longest x1 1.65 us: shards(): gated_in = (glu_value.astype(jnp.float32) * jax.nn.sigmoid(glu_gate.astyp...]
  transfers between devices with their start and end apart: 2 -> 0, of which waited for: 1 -> 0; matrix products, arithmetic and copies ran while one was open for 1% -> 0% of each run, Pallas kernels for 0% -> 0%
where the time goes in v3:
time: 188 us; the launch traced here: 187 us
  Pallas kernels  185 us (98%)
    pallas_call x1, Pallas kernels, shards(): pl.pallas_call(layer_kernel, out_shape=jax.ShapeDtypeStruct((BLOCK, width...  185 us

profile of v3, /device:TPU:1, one launch (start us, length us, event | category | flops | bytes accessed | tf_op | source)
XLA Modules:
  0.0 187.4 jit_solution(7175273158466628613)
XLA Ops:
  0.0 185.5 %layer.1 = bf16[128,2048]{1,0:T(8,128)(2,1)} custom-call(bf16[512,512]{1,0:T(8,128)(2,1)} %value.1, bf16[512,512]{1,0:T(8,128)(2,1)} %gate.1, f32[31,512]{1,0:T(8,128)} %taps.1, f32[1,512]{1,0:T(1,128)} %bitcast.7, bf16[128,2048]{1,0:T(8,128)(2,1)} %residual.1, f32[1,2048]{1,0:T(1,128)} %bitcast.5, f32[1,2048]{1,0:T(1,128)} %bitcast.6, s32[2,128]{1,0:T(2,128)} %bitcast.8, ...), custom_call_target="tpu_custom_call" | custom-call | tf_op jit(solution)/shard_map/layer/pallas_call | solution.py:477
  185.5 1.9 %copy.15 = bf16[128,2048]{1,0:T(8,128)(2,1)} copy(bf16[128,2048]{1,0:T(8,128)(2,1)} %layer.1) | data formatting | bytes 1048576

commit v4 on v3

--- a/solution.py
+++ b/solution.py
@@ -12,10 +12,13 @@
 Z, Y, CORES, N_TP = 8, 4, 2, 4
 PLANE = Y * CORES
 N_SP = Z * PLANE
-GROUPS = 4
-PEERS = 2 * PLANE
-SELF_GROUP = 3
-SELF = SELF_GROUP * PEERS + PLANE
+BANDS = 4
+GROUPS = 2 * BANDS
+AHEAD = 3
+SIDE = PLANE // 2
+PEERS = 2 * SIDE
+SELF_GROUP = 2
+SELF = SELF_GROUP * PEERS + SIDE
 CAP = 8
 TILE = 256
 LANES = 128
@@ -43,8 +46,9 @@
     return sp, tp, z, y, core, weight_partner, row_partner
 
 
-def step_along_z(group, half):
-    return (group + 1) if half == 0 else (7 - group) * (1 - (group + 1) // 4)
+def step_along_z(band, half):
+    distance = 3 + band - 3 * (band // 2) - 2 * (band // 3)
+    return distance if half == 0 else (Z - distance) * (1 - distance // 4)
 
 
 def peer_at(z, y, core, dz, r, sign):
@@ -56,10 +60,9 @@
 
 
 def layer_kernel(
-    value, gate, taps, norm_gain, residual, resid_gain, out_gain, ids, weights,
-    mix_weight, w_gate, w_up, w_down,
+    value_h, gate_h, taps_h, norm_gain_h, residual_h, resid_gain_h, out_gain_h, ids_h, weights_h, mix_weight, w_gate, w_up, w_down,
     out,
-    ext, halo_send, halo_recv, conv_v, stat_cols, stat_rows, stats_send, stats_recv, mix_in, mix_v,
+    value, gate, taps, norm_gain, residual, resid_gain, out_gain, ids, weights, total_v, ext, halo_send, halo_recv, conv_v, stat_cols, stat_rows, stats_send, stats_recv, mix_in, mix_v,
     a_send_v, a_recv_v, b_send_v, b_recv_v, acc, hidden, held, share, slots, ret,
     gate_v, up_v, down_v, recv, xrecv, rows_v, act_v, kept, xsend, xret, fin,
     d_send, d_recv, x_send, x_recv, b_send, b_recv, r_send, r_recv, w_send, w_recv, l_sem,
@@ -79,14 +82,23 @@
     width = w_down.shape[2]
     half_units = w_down.shape[1]
     channels = value.shape[1]
+    first_loads = [
+        pltpu.make_async_copy(src, dst, l_sem.at[4 + i])
+        for i, (src, dst) in enumerate([
+            (value_h, value), (gate_h, gate), (taps_h, taps), (norm_gain_h, norm_gain),
+            (residual_h, residual), (resid_gain_h, resid_gain), (out_gain_h, out_gain), (ids_h, ids), (weights_h, weights),
+        ])
+    ]
     loads = [
         pltpu.make_async_copy(mix_weight, mix_v, l_sem.at[3]),
         pltpu.make_async_copy(w_gate.at[0], gate_v.at[0], l_sem.at[0]),
         pltpu.make_async_copy(w_up.at[0], up_v.at[0], l_sem.at[1]),
         pltpu.make_async_copy(w_down.at[0], down_v.at[0:half_units], l_sem.at[2]),
     ]
-    for load in loads:
+    for load in first_loads + loads:
         load.start()
+    for load in first_loads[:2]:
+        load.wait()
 
     lane_groups = channels // LANES
 
@@ -105,6 +117,8 @@
         return 0
 
     lax.fori_loop(0, ROWS // STRIPE, gate_rows, 0)
+    for load in first_loads[2:]:
+        load.wait()
     pl.semaphore_wait(barrier, N_SP - 1 + N_TP - 1)
     halo_copy = pltpu.make_async_remote_copy(
         src_ref=halo_send, dst_ref=halo_recv, send_sem=h_sem.at[0], recv_sem=h_sem.at[1],
@@ -121,7 +135,7 @@
     def rows_of(ref, first, last):
         return ref.at[pl.ds(first, last - first)]
 
-    cuts = (0, 512, 1024, 2048)
+    cuts = (0, 768, 1536, 2048)
     swaps = [
         swap(i, w_gate.at[0, pl.ds(f, l - f)], gate_v.at[1, pl.ds(f, l - f)])
         for i, (f, l) in enumerate(zip(cuts, cuts[1:]))
@@ -175,7 +189,11 @@
     one = [(spot == ids[j : j + 1, :]).astype(BF16) for j in range(2)]
     before = lax.broadcasted_iota(jnp.int32, (BLOCK, BLOCK), 0) < lax.broadcasted_iota(jnp.int32, (BLOCK, BLOCK), 1)
     earlier = jnp.dot(one[0] + one[1], before.astype(BF16), preferred_element_type=F32)
-    owner = lax.broadcasted_iota(jnp.int32, (experts * CAP, experts), 0) // CAP
+    place = lax.broadcasted_iota(jnp.int32, (experts * CAP, experts), 0) // CAP
+    group = place // PEERS
+    band, r = group // 2, (group % 2) * SIDE + place % SIDE
+    step = jnp.where((place // SIDE) % 2 == 0, step_along_z(band, 0), step_along_z(band, 1))
+    owner = peer_at(z, y, core, step, r, 1)
     spread_out = (owner == lax.broadcasted_iota(jnp.int32, (experts * CAP, experts), 1)).astype(BF16)
     rank = jnp.dot(spread_out, earlier.astype(BF16), preferred_element_type=F32)
     in_rank = rank == (lax.broadcasted_iota(jnp.int32, (experts * CAP, BLOCK), 0) % CAP).astype(F32)
@@ -289,35 +307,47 @@
             acc[h, at] + b_recv_v[0, h, at].astype(F32) + b_recv_v[1, h, at].astype(F32) for h in range(2)
         ]
         total = jnp.concatenate(halves, axis=1) + residual[at].astype(F32)
-        hidden[at] = normalize(total, resid_gain[...]).astype(BF16)
-        return 0
-
-    lax.fori_loop(0, BLOCK // strip, norm_rows, 0)
-
-    def fill_slots(n, _):
-        cols = pl.ds(pl.multiple_of(n * TILE, TILE), TILE)
-        picked = jnp.dot(held[...], hidden[:, cols], preferred_element_type=F32)
-        slots[:, :, cols] = picked.reshape(experts, CAP, TILE).astype(BF16)
-        return 0
-
-    lax.fori_loop(0, width // TILE, fill_slots, 0)
-
-    pltpu.make_async_copy(slots.at[sp], recv.at[SELF], d_recv.at[SELF]).start()
+        rows = normalize(total, resid_gain[...]).astype(BF16)
+        hidden[at] = rows
+        total_v[at] = rows.astype(F32)
+        return 0
+
+    lax.fori_loop(0, BLOCK // strip, norm_rows, 0, unroll=True)
+
+    band_slots = 2 * PEERS * CAP
+
+    def fill_slots(band):
+        at = slice(band * band_slots, (band + 1) * band_slots)
+
+        def one_tile(n, _):
+            cols = pl.ds(pl.multiple_of(n * TILE, TILE), TILE)
+            picked = jnp.dot(held[at, :], hidden[:, cols], preferred_element_type=F32)
+            to = slice(band * 2 * PEERS, (band + 1) * 2 * PEERS)
+            slots[to, :, cols] = picked.reshape(2 * PEERS, CAP, TILE).astype(BF16)
+            return 0
+
+        lax.fori_loop(0, width // TILE, one_tile, 0)
+
     for group in range(GROUPS):
+        if group % 2 == 0:
+            fill_slots(group // 2)
+        if group == SELF_GROUP:
+            pltpu.make_async_copy(slots.at[SELF], recv.at[SELF], d_recv.at[SELF]).start()
         for half in range(2):
-            dz = step_along_z(group, half)
-            base = group * PEERS + half * PLANE
-
-            def send(r, _, dz=dz, base=base):
-                other = peer_at(z, y, core, dz, r, 1)
+            dz = step_along_z(group // 2, half)
+            base = group * PEERS + half * SIDE
+
+            def send(r, _, dz=dz, base=base, group=group):
+                other = peer_at(z, y, core, dz, (group % 2) * SIDE + r, 1)
                 pltpu.make_async_remote_copy(
-                    src_ref=slots.at[other], dst_ref=recv.at[base + r],
+                    src_ref=slots.at[base + r], dst_ref=recv.at[base + r],
                     send_sem=d_send.at[base + r], recv_sem=d_recv.at[base + r],
                     device_id=(other, tp), device_id_type=MESH,
                 ).start()
                 return 0
 
-            lax.fori_loop(1 if base == SELF else 0, PLANE, send, 0)
+            lax.fori_loop(1 if base == SELF else 0, SIDE, send, 0)
+
     def cross(c, src, dst, send_sem, recv_sem):
         return pltpu.make_async_remote_copy(
             src_ref=src.at[pl.ds(c * PEERS, PEERS)], dst_ref=dst.at[pl.ds(c * PEERS, PEERS)],
@@ -325,97 +355,138 @@
             device_id=(sp, row_partner), device_id_type=MESH,
         )
 
+    def cross_back(c, half):
+        at, cols = pl.ds(c * PEERS, PEERS), pl.ds(half * half_width, half_width)
+        return pltpu.make_async_remote_copy(
+            src_ref=xsend.at[at, :, cols], dst_ref=xret.at[at, :, cols],
+            send_sem=b_send.at[2 * c + half], recv_sem=b_recv.at[2 * c + half],
+            device_id=(sp, row_partner), device_id_type=MESH,
+        )
+
     count = PEERS * CAP
 
-    def stage(step, _):
-        @pl.when(step < GROUPS)
-        def arrive():
-            def one(r, _):
-                wait_for(recv.at[step * PEERS + r], d_recv.at[step * PEERS + r])
+    def arrive(group):
+        def one(r, _):
+            wait_for(recv.at[group * PEERS + r], d_recv.at[group * PEERS + r])
+            return 0
+
+        lax.fori_loop(0, PEERS, one, 0)
+        cross(group, recv, xrecv, x_send, x_recv).start()
+
+    def compute(c):
+        cross(c, recv, xrecv, x_send, x_recv).wait_recv()
+        at = pl.ds(c * PEERS, PEERS)
+        rows_v[0:count] = recv[at].astype(F32).reshape(count, width).astype(BF16)
+        rows_v[count : 2 * count] = xrecv[at].astype(F32).reshape(count, width).astype(BF16)
+
+        def activate(j, _):
+            half, col = j // 2, pl.multiple_of((j % 2) * TILE, TILE)
+            g = jnp.dot(rows_v[...], gate_v[half, :, pl.ds(col, TILE)], preferred_element_type=F32)
+            u = jnp.dot(rows_v[...], up_v[half, :, pl.ds(col, TILE)], preferred_element_type=F32)
+            g = jnp.minimum(g, LIMIT)
+            u = jnp.clip(u, -LIMIT, LIMIT)
+            act = (u + 1.0) * g * jax.nn.sigmoid(SLOPE * g)
+            act_v[:, pl.ds(pl.multiple_of(j * TILE, TILE), TILE)] = act.astype(BF16)
+            return 0
+
+        lax.fori_loop(0, 2 * half_units // TILE, activate, 0)
+
+        @pl.when(c == 0)
+        def down_weights():
+            swaps[-1].wait_recv()
+
+        def project(n, _):
+            cols = pl.ds(pl.multiple_of(n * TILE, TILE), TILE)
+            result = jnp.dot(act_v[...], down_v[:, cols], preferred_element_type=F32)
+            kept[c % 2, :, cols] = result[0:count]
+            xsend[at, :, cols] = result[count : 2 * count].reshape(PEERS, CAP, TILE).astype(BF16)
+            return 0
+
+        tiles = half_width // TILE
+        for half in range(2):
+            lax.fori_loop(half * tiles, (half + 1) * tiles, project, 0)
+            cross_back(c, half).start()
+
+    def give_back(c):
+        at = pl.ds(c * PEERS, PEERS)
+        for half in range(2):
+            cross_back(c, half).wait_recv()
+        total = kept[c % 2].reshape(PEERS, CAP, width) + xret[at].astype(F32)
+        fin[at] = total.astype(BF16)
+        for half in range(2):
+            dz = step_along_z(c // 2, half)
+
+            def send(r, _, dz=dz, half=half):
+                k = c * PEERS + half * SIDE + r
+                other = peer_at(z, y, core, dz, (c % 2) * SIDE + r, -1)
+
+                @pl.when(k != SELF)
+                def away():
+                    pltpu.make_async_remote_copy(
+                        src_ref=fin.at[k], dst_ref=ret.at[k],
+                        send_sem=r_send.at[k], recv_sem=r_recv.at[k],
+                        device_id=(other, tp), device_id_type=MESH,
+                    ).start()
+
+                @pl.when(k == SELF)
+                def here():
+                    pltpu.make_async_copy(fin.at[k], ret.at[k], r_recv.at[k]).start()
+
                 return 0
 
-            lax.fori_loop(0, PEERS, one, 0)
-            cross(step, recv, xrecv, x_send, x_recv).start()
-
-        @pl.when(step == 0)
-        def gate_weights():
-            for load in loads[1:]:
-                load.wait()
-            for s in swaps[:-1]:
-                s.wait_recv()
-
-        @pl.when((step >= 1) & (step <= GROUPS))
-        def compute():
-            c = step - 1
-            cross(c, recv, xrecv, x_send, x_recv).wait_recv()
-            at = pl.ds(c * PEERS, PEERS)
-            rows_v[0:count] = recv[at].astype(jnp.float32).reshape(count, width).astype(jnp.bfloat16)
-            rows_v[count : 2 * count] = xrecv[at].astype(jnp.float32).reshape(count, width).astype(jnp.bfloat16)
-
-            def activate(j, _):
-                half, col = j // 2, pl.multiple_of((j % 2) * TILE, TILE)
-                g = jnp.dot(rows_v[...], gate_v[half, :, pl.ds(col, TILE)], preferred_element_type=jnp.float32)
-                u = jnp.dot(rows_v[...], up_v[half, :, pl.ds(col, TILE)], preferred_element_type=jnp.float32)
-                g = jnp.minimum(g, LIMIT)
-                u = jnp.clip(u, -LIMIT, LIMIT)
-                act = (u + 1.0) * g * jax.nn.sigmoid(SLOPE * g)
-                act_v[:, pl.ds(pl.multiple_of(j * TILE, TILE), TILE)] = act.astype(jnp.bfloat16)
-                return 0
-
-            lax.fori_loop(0, 2 * half_units // TILE, activate, 0)
-
-            @pl.when(step == 1)
-            def down_weights():
-                swaps[-1].wait_recv()
-
-
-            def project(n, _):
-                cols = pl.ds(pl.multiple_of(n * TILE, TILE), TILE)
-                out = jnp.dot(act_v[...], down_v[:, cols], preferred_element_type=jnp.float32)
-                kept[c % 2, :, cols] = out[0:count]
-                xsend[at, :, cols] = out[count : 2 * count].reshape(PEERS, CAP, TILE).astype(jnp.bfloat16)
-                return 0
-
-            lax.fori_loop(0, width // TILE, project, 0)
-            cross(c, xsend, xret, b_send, b_recv).start()
-
-        @pl.when(step >= 2)
-        def give_back():
-            c = step - 2
-            cross(c, xsend, xret, b_send, b_recv).wait_recv()
-            at = pl.ds(c * PEERS, PEERS)
-            total = kept[c % 2].reshape(PEERS, CAP, width) + xret[at].astype(jnp.float32)
-            fin[at] = total.astype(jnp.bfloat16)
-            for half in range(2):
-                dz = step_along_z(c, half)
-
-                def send(r, _, dz=dz, half=half):
-                    k = c * PEERS + half * PLANE + r
-                    other = peer_at(z, y, core, dz, r, -1)
-
-                    @pl.when(k != SELF)
-                    def away():
-                        pltpu.make_async_remote_copy(
-                            src_ref=fin.at[k], dst_ref=ret.at[sp],
-                            send_sem=r_send.at[k], recv_sem=r_recv.at[k],
-                            device_id=(other, tp), device_id_type=MESH,
-                        ).start()
-
-                    @pl.when(k == SELF)
-                    def here():
-                        pltpu.make_async_copy(fin.at[k], ret.at[sp], r_recv.at[k]).start()
-
-                    return 0
-
-                lax.fori_loop(0, PLANE, send, 0)
-
-        return 0
-
-    lax.fori_loop(0, GROUPS + 2, stage, 0)
-
-    def finish(k, _):
-        wait_for(ret.at[k], r_recv.at[k])
-
+            lax.fori_loop(0, SIDE, send, 0)
+
+    arrive(0)
+    for load in loads[1:]:
+        load.wait()
+    for s in swaps[:-1]:
+        s.wait_recv()
+
+    def stage(c, _):
+        @pl.when(c == 1)
+        def early():
+            give_back(0)
+
+        compute(c)
+
+        @pl.when(c == 0)
+        def next_rows():
+            for group in range(1, AHEAD):
+                arrive(group)
+
+        @pl.when(c < GROUPS - AHEAD)
+        def later_rows():
+            arrive(c + AHEAD)
+
+        @pl.when(c >= 2)
+        def late():
+            give_back(c - 1)
+
+        return 0
+
+    def gather_band(band, _):
+        def one(r, _):
+            wait_for(ret.at[band * 2 * PEERS + r], r_recv.at[band * 2 * PEERS + r])
+            return 0
+
+        lax.fori_loop(0, 2 * PEERS, one, 0)
+        own = share[:, pl.ds(pl.multiple_of(band * band_slots, band_slots), band_slots)]
+
+        def one_tile(n, _):
+            cols = pl.ds(pl.multiple_of(n * TILE, TILE), TILE)
+            rows = ret[pl.ds(band * 2 * PEERS, 2 * PEERS), :, cols].astype(F32).reshape(band_slots, TILE).astype(BF16)
+            both = jnp.dot(own, rows, preferred_element_type=F32)
+            total_v[:, cols] += both[0:BLOCK] + both[BLOCK : 2 * BLOCK]
+            return 0
+
+        lax.fori_loop(0, width // TILE, one_tile, 0)
+        return 0
+
+    lax.fori_loop(0, GROUPS, stage, 0)
+    lax.fori_loop(0, BANDS - 2, gather_band, 0)
+    give_back(GROUPS - 1)
+
+    def sent(k, _):
         @pl.when(k != SELF)
         def away():
             wait_for(recv.at[k], d_send.at[k])
@@ -423,31 +494,22 @@
 
         return 0
 
-    lax.fori_loop(0, Z * PLANE, finish, 0)
+    lax.fori_loop(BANDS - 2, BANDS - 1, gather_band, 0)
+    lax.fori_loop(0, N_SP, sent, 0)
     for c in range(GROUPS):
         cross(c, recv, xrecv, x_send, x_recv).wait_send()
-        cross(c, xsend, xret, b_send, b_recv).wait_send()
+        for half in range(2):
+            cross_back(c, half).wait_send()
     for copy in [halo_copy, *swaps, *stat_copies, *far_copies, *near_copies[0], *near_copies[1]]:
         copy.wait_send()
-
-    def gather_rows(n, _):
-        cols = pl.ds(pl.multiple_of(n * TILE, TILE), TILE)
-        rows = ret[:, :, cols].astype(F32).reshape(experts * CAP, TILE).astype(BF16)
-        both = jnp.dot(share[...], rows, preferred_element_type=F32)
-        half = n // (half_width // TILE)
-        to = pl.ds(pl.multiple_of(n * TILE - half * half_width, TILE), TILE)
-        acc[half, :, to] = both[0:BLOCK] + both[BLOCK : 2 * BLOCK] + hidden[:, cols].astype(F32)
-        return 0
-
-    lax.fori_loop(0, width // TILE, gather_rows, 0)
+    gather_band(BANDS - 1, 0)
 
     def last_norm(i, _):
         at = pl.ds(pl.multiple_of(i * strip, strip), strip)
-        total = jnp.concatenate([acc[0, at], acc[1, at]], axis=1)
-        out[at] = normalize(total, out_gain[...]).astype(BF16)
-        return 0
-
-    lax.fori_loop(0, BLOCK // strip, last_norm, 0)
+        out[at] = normalize(total_v[at], out_gain[...]).astype(BF16)
+        return 0
+
+    lax.fori_loop(0, BLOCK // strip, last_norm, 0, unroll=True)
 
 
 def shards(
@@ -472,14 +534,24 @@
     experts = N_SP
     count = PEERS * CAP
     dma = pltpu.SemaphoreType.DMA
-    vmem, hbm = pl.BlockSpec(memory_space=pltpu.VMEM), pl.BlockSpec(memory_space=pl.ANY)
+    vmem, hbm = pl.BlockSpec(memory_space=pltpu.VMEM), pl.BlockSpec(memory_space=pltpu.MemorySpace.HBM)
     moved = pltpu.VMEM((experts, CAP, width), BF16)
     return pl.pallas_call(
         layer_kernel,
         out_shape=jax.ShapeDtypeStruct((BLOCK, width), BF16),
-        in_specs=[vmem] * 9 + [hbm] * 4,
+        in_specs=[hbm] * 13,
         out_specs=vmem,
         scratch_shapes=[
+            pltpu.VMEM(glu_value.shape, BF16),
+            pltpu.VMEM(glu_gate.shape, BF16),
+            pltpu.VMEM(conv_kernel.shape, F32),
+            pltpu.VMEM((1, channels), F32),
+            pltpu.VMEM(residual.shape, BF16),
+            pltpu.VMEM((1, width), F32),
+            pltpu.VMEM((1, width), F32),
+            pltpu.VMEM((2, BLOCK), jnp.int32),
+            pltpu.VMEM((2, BLOCK), F32),
+            pltpu.VMEM((BLOCK, width), F32),
             pltpu.VMEM((groups, ROWS + HALO, LANES), F32),
             pltpu.VMEM((groups, HALO, LANES), BF16),
             pltpu.VMEM((groups, HALO, LANES), BF16),
@@ -513,9 +585,9 @@
             moved,
             dma((experts,)), dma((experts,)),
             dma((GROUPS,)), dma((GROUPS,)),
-            dma((GROUPS,)), dma((GROUPS,)),
+            dma((2 * GROUPS,)), dma((2 * GROUPS,)),
             dma((experts,)), dma((experts,)),
-            dma((5,)), dma((5,)), dma((4,)),
+            dma((5,)), dma((5,)), dma((13,)),
             dma((2,)), dma((3,)), dma((3,)),
             dma((2,)), dma((2,)), dma((4,)), dma((4,)),
         ],

time: 188 us -> 169 us (0.90)
  Pallas kernels: 185 us -> 167 us
    pallas_call x1, Pallas kernels: 185 us -> 167 us  [shards(): pl.pallas_call(layer_kernel, out_shape=jax.ShapeDtypeStruct((BLOCK, width...]
where the time goes in v4:
time: 169 us
  Pallas kernels  167 us (99%)
  local copies, waits for them, and re-layouts  1.88 us (1%)
    pallas_call x1, Pallas kernels, shards(): pl.pallas_call(layer_kernel, out_shape=jax.ShapeDtypeStruct((BLOCK, width...  167 us

profile of v4, /device:TPU:1, one launch (start us, length us, event | category | flops | bytes accessed | tf_op | source)
XLA Modules:
  0.0 168.6 jit_solution(5597428776879479215)
XLA Ops:
  0.0 166.7 %layer.1 = bf16[128,2048]{1,0:T(8,128)(2,1)} custom-call(bf16[512,512]{1,0:T(8,128)(2,1)} %value_h.1, bf16[512,512]{1,0:T(8,128)(2,1)} %gate_h.1, f32[31,512]{1,0:T(8,128)} %taps_h.1, f32[1,512]{1,0:T(1,128)} %bitcast.7, bf16[128,2048]{1,0:T(8,128)(2,1)} %residual_h.1, f32[1,2048]{1,0:T(1,128)} %bitcast.5, f32[1,2048]{1,0:T(1,128)} %bitcast.6, ...), custom_call_target="tpu_custom_call" | custom-call | tf_op jit(solution)/shard_map/layer/pallas_call | solution.py:539
  166.7 1.9 %copy.15 = bf16[128,2048]{1,0:T(8,128)(2,1)} copy(bf16[128,2048]{1,0:T(8,128)(2,1)} %layer.1) | data formatting | bytes 1048576

commit v5 on v4

--- a/solution.py
+++ b/solution.py
@@ -14,10 +14,10 @@
 N_SP = Z * PLANE
 BANDS = 4
 GROUPS = 2 * BANDS
-AHEAD = 3
+FIRST = 2
 SIDE = PLANE // 2
 PEERS = 2 * SIDE
-SELF_GROUP = 2
+SELF_GROUP = 3
 SELF = SELF_GROUP * PEERS + SIDE
 CAP = 8
 TILE = 256
@@ -66,21 +66,32 @@
     a_send_v, a_recv_v, b_send_v, b_recv_v, acc, hidden, held, share, slots, ret,
     gate_v, up_v, down_v, recv, xrecv, rows_v, act_v, kept, xsend, xret, fin,
     d_send, d_recv, x_send, x_recv, b_send, b_recv, r_send, r_recv, w_send, w_recv, l_sem,
-    h_sem, s_send, s_recv, ra_send, ra_recv, rb_send, rb_recv,
+    word, h_sem, s_send, s_recv, ra_send, ra_recv, rb_send, rb_recv,
 ):
     sp, tp, z, y, core, weight_partner, row_partner = position()
     barrier = pltpu.get_barrier_semaphore()
 
-    def greet(i, _):
-        other = lax.rem(sp + i, N_SP)
+    along_z = [((z + d) % Z) * PLANE + sp % PLANE for d in (1, Z - 1)]
+    along_y = [z * PLANE + ((y + d) % Y) * CORES + core for d in (1, Y - 1)]
+    along_sp = [(sp + d) % N_SP for d in (1, N_SP - 1)]
+    for other in along_sp + along_z + along_y:
         pl.semaphore_signal(barrier, inc=1, device_id=(other, tp), device_id_type=MESH)
-        return 0
-
-    lax.fori_loop(1, N_SP, greet, 0)
     for i in range(1, N_TP):
         pl.semaphore_signal(barrier, inc=1, device_id=(sp, (tp + i) % N_TP), device_id_type=MESH)
+    rounds = [along_z] * 3 + [along_y] * 2 + [[z * PLANE + y * CORES + 1 - core]]
+
+    def tell(i):
+        for other in rounds[i]:
+            pl.semaphore_signal(word.at[i], inc=1, device_id=(other, tp), device_id_type=MESH)
+
+    def hear(i):
+        pl.semaphore_wait(word.at[i], len(rounds[i]))
+        if i + 1 < len(rounds):
+            tell(i + 1)
+
     width = w_down.shape[2]
     half_units = w_down.shape[1]
+    half_width = width // 2
     channels = value.shape[1]
     first_loads = [
         pltpu.make_async_copy(src, dst, l_sem.at[4 + i])
@@ -119,7 +130,8 @@
     lax.fori_loop(0, ROWS // STRIPE, gate_rows, 0)
     for load in first_loads[2:]:
         load.wait()
-    pl.semaphore_wait(barrier, N_SP - 1 + N_TP - 1)
+    pl.semaphore_wait(barrier, 6 + N_TP - 1)
+    tell(0)
     halo_copy = pltpu.make_async_remote_copy(
         src_ref=halo_send, dst_ref=halo_recv, send_sem=h_sem.at[0], recv_sem=h_sem.at[1],
         device_id=(lax.rem(sp + 1, N_SP), tp), device_id_type=MESH,
@@ -141,7 +153,12 @@
         for i, (f, l) in enumerate(zip(cuts, cuts[1:]))
     ] + [
         swap(3, w_up.at[0], up_v.at[1]),
-        swap(4, w_down.at[0], down_v.at[half_units : 2 * half_units]),
+    ] + [
+        swap(
+            4 + h, w_down.at[0, :, pl.ds(h * half_width, half_width)],
+            down_v.at[pl.ds(half_units, half_units), pl.ds(h * half_width, half_width)],
+        )
+        for h in range(2)
     ]
     swaps[0].start()
 
@@ -166,6 +183,7 @@
         return 0
 
     lax.fori_loop(1, ROWS // STRIPE, convolve_step, 0)
+    hear(0)
     halo_copy.wait_recv()
     for g in range(lane_groups):
         ext[g, 0:HALO] = jnp.where(sp > 0, halo_recv[g].astype(F32), 0.0)
@@ -184,6 +202,8 @@
         c.start()
     swaps[1].start()
 
+    hear(1)
+
     experts = N_SP
     spot = lax.broadcasted_iota(jnp.int32, (experts, BLOCK), 0)
     one = [(spot == ids[j : j + 1, :]).astype(BF16) for j in range(2)]
@@ -191,7 +211,7 @@
     earlier = jnp.dot(one[0] + one[1], before.astype(BF16), preferred_element_type=F32)
     place = lax.broadcasted_iota(jnp.int32, (experts * CAP, experts), 0) // CAP
     group = place // PEERS
-    band, r = group // 2, (group % 2) * SIDE + place % SIDE
+    band, r = group // 2, (1 - group % 2) * SIDE + place % SIDE
     step = jnp.where((place // SIDE) % 2 == 0, step_along_z(band, 0), step_along_z(band, 1))
     owner = peer_at(z, y, core, step, r, 1)
     spread_out = (owner == lax.broadcasted_iota(jnp.int32, (experts * CAP, experts), 1)).astype(BF16)
@@ -209,6 +229,7 @@
         share[0:BLOCK, at] = high
         share[BLOCK : 2 * BLOCK, at] = (part - high.astype(F32)).astype(BF16)
     stat_rows[...] = jnp.zeros_like(stat_rows)
+    hear(2)
 
     for c in stat_copies:
         c.wait_recv()
@@ -227,8 +248,6 @@
             lanes = slice(g * LANES, (g + 1) * LANES)
             v = (conv_v[g, at] - columns[:, 0:1]) * columns[:, 1:2] * norm_gain[:, lanes]
             mix_in[at, lanes] = (v / (1.0 + jnp.exp(-v))).astype(BF16)
-
-    half_width = width // 2
 
     def project_rows(b, half, into):
         at = pl.ds(pl.multiple_of(b * BLOCK, BLOCK), BLOCK)
@@ -259,6 +278,7 @@
         ]
         for i in range(2)
     ]
+    hear(3)
     far = (tp + 2) % N_TP
     sides = [(tp + 1) % N_TP, (tp + N_TP - 1) % N_TP]
     mix_rows(far)
@@ -287,6 +307,7 @@
         near_copies[i][i].start()
     for s in swaps[2:]:
         s.start()
+    hear(4)
     mix_rows(tp)
     for h in range(2):
 
@@ -312,6 +333,7 @@
         total_v[at] = rows.astype(F32)
         return 0
 
+    hear(5)
     lax.fori_loop(0, BLOCK // strip, norm_rows, 0, unroll=True)
 
     band_slots = 2 * PEERS * CAP
@@ -338,7 +360,7 @@
             base = group * PEERS + half * SIDE
 
             def send(r, _, dz=dz, base=base, group=group):
-                other = peer_at(z, y, core, dz, (group % 2) * SIDE + r, 1)
+                other = peer_at(z, y, core, dz, (1 - group % 2) * SIDE + r, 1)
                 pltpu.make_async_remote_copy(
                     src_ref=slots.at[base + r], dst_ref=recv.at[base + r],
                     send_sem=d_send.at[base + r], recv_sem=d_recv.at[base + r],
@@ -373,7 +395,7 @@
         lax.fori_loop(0, PEERS, one, 0)
         cross(group, recv, xrecv, x_send, x_recv).start()
 
-    def compute(c):
+    def activations(c):
         cross(c, recv, xrecv, x_send, x_recv).wait_recv()
         at = pl.ds(c * PEERS, PEERS)
         rows_v[0:count] = recv[at].astype(F32).reshape(count, width).astype(BF16)
@@ -386,90 +408,59 @@
             g = jnp.minimum(g, LIMIT)
             u = jnp.clip(u, -LIMIT, LIMIT)
             act = (u + 1.0) * g * jax.nn.sigmoid(SLOPE * g)
-            act_v[:, pl.ds(pl.multiple_of(j * TILE, TILE), TILE)] = act.astype(BF16)
+            act_v[c, :, pl.ds(pl.multiple_of(j * TILE, TILE), TILE)] = act.astype(BF16)
             return 0
 
         lax.fori_loop(0, 2 * half_units // TILE, activate, 0)
 
-        @pl.when(c == 0)
-        def down_weights():
-            swaps[-1].wait_recv()
+    def outputs(c, half):
+        at = pl.ds(c * PEERS, PEERS)
 
         def project(n, _):
-            cols = pl.ds(pl.multiple_of(n * TILE, TILE), TILE)
-            result = jnp.dot(act_v[...], down_v[:, cols], preferred_element_type=F32)
-            kept[c % 2, :, cols] = result[0:count]
+            cols = pl.ds(pl.multiple_of(half * half_width + n * TILE, TILE), TILE)
+            result = jnp.dot(act_v[c], down_v[:, cols], preferred_element_type=F32)
+            kept[c, :, cols] = result[0:count]
             xsend[at, :, cols] = result[count : 2 * count].reshape(PEERS, CAP, TILE).astype(BF16)
             return 0
 
-        tiles = half_width // TILE
-        for half in range(2):
-            lax.fori_loop(half * tiles, (half + 1) * tiles, project, 0)
-            cross_back(c, half).start()
-
-    def give_back(c):
-        at = pl.ds(c * PEERS, PEERS)
-        for half in range(2):
-            cross_back(c, half).wait_recv()
-        total = kept[c % 2].reshape(PEERS, CAP, width) + xret[at].astype(F32)
-        fin[at] = total.astype(BF16)
-        for half in range(2):
-            dz = step_along_z(c // 2, half)
-
-            def send(r, _, dz=dz, half=half):
-                k = c * PEERS + half * SIDE + r
-                other = peer_at(z, y, core, dz, (c % 2) * SIDE + r, -1)
+        lax.fori_loop(0, half_width // TILE, project, 0)
+        cross_back(c, half).start()
+
+    def give_back(c, h):
+        at, cols = pl.ds(c * PEERS, PEERS), pl.ds(pl.multiple_of(h * half_width, half_width), half_width)
+        cross_back(c, h).wait_recv()
+        total = kept[c, :, cols].reshape(PEERS, CAP, half_width) + xret[at, :, cols].astype(F32)
+        fin[at, :, cols] = total.astype(BF16)
+        for side in range(2):
+            dz = step_along_z(c // 2, side)
+
+            def send(r, _, dz=dz, side=side):
+                k = c * PEERS + side * SIDE + r
+                other = peer_at(z, y, core, dz, (1 - c % 2) * SIDE + r, -1)
 
                 @pl.when(k != SELF)
                 def away():
                     pltpu.make_async_remote_copy(
-                        src_ref=fin.at[k], dst_ref=ret.at[k],
-                        send_sem=r_send.at[k], recv_sem=r_recv.at[k],
+                        src_ref=fin.at[k, :, cols], dst_ref=ret.at[k, :, cols],
+                        send_sem=r_send.at[2 * k + h], recv_sem=r_recv.at[2 * k + h],
                         device_id=(other, tp), device_id_type=MESH,
                     ).start()
 
                 @pl.when(k == SELF)
                 def here():
-                    pltpu.make_async_copy(fin.at[k], ret.at[k], r_recv.at[k]).start()
+                    pltpu.make_async_copy(fin.at[k, :, cols], ret.at[k, :, cols], r_recv.at[2 * k + h]).start()
 
                 return 0
 
             lax.fori_loop(0, SIDE, send, 0)
-
-    arrive(0)
-    for load in loads[1:]:
-        load.wait()
-    for s in swaps[:-1]:
-        s.wait_recv()
-
-    def stage(c, _):
-        @pl.when(c == 1)
-        def early():
-            give_back(0)
-
-        compute(c)
-
-        @pl.when(c == 0)
-        def next_rows():
-            for group in range(1, AHEAD):
-                arrive(group)
-
-        @pl.when(c < GROUPS - AHEAD)
-        def later_rows():
-            arrive(c + AHEAD)
-
-        @pl.when(c >= 2)
-        def late():
-            give_back(c - 1)
-
-        return 0
 
     def gather_band(band, _):
         def one(r, _):
-            wait_for(ret.at[band * 2 * PEERS + r], r_recv.at[band * 2 * PEERS + r])
+            k = band * 2 * PEERS + r // 2
+            wait_for(ret.at[k, :, pl.ds(0, half_width)], r_recv.at[2 * k + r % 2])
             return 0
 
-        lax.fori_loop(0, 2 * PEERS, one, 0)
+        lax.fori_loop(0, 4 * PEERS, one, 0)
         own = share[:, pl.ds(pl.multiple_of(band * band_slots, band_slots), band_slots)]
 
         def one_tile(n, _):
@@ -482,27 +473,82 @@
         lax.fori_loop(0, width // TILE, one_tile, 0)
         return 0
 
-    lax.fori_loop(0, GROUPS, stage, 0)
-    lax.fori_loop(0, BANDS - 2, gather_band, 0)
-    give_back(GROUPS - 1)
-
-    def sent(k, _):
-        @pl.when(k != SELF)
-        def away():
-            wait_for(recv.at[k], d_send.at[k])
-            wait_for(fin.at[k], r_send.at[k])
+    def unit_of(u):
+        early = u < 2 * FIRST
+        return jnp.where(early, u % FIRST, u // 2), jnp.where(early, u // FIRST, u % 2)
+
+    arrive(0)
+    for load in loads[1:]:
+        load.wait()
+    for s in swaps[:4]:
+        s.wait_recv()
+    arrive(1)
+
+    def stage(u, _):
+        c, h = unit_of(u)
+
+        @pl.when((u == FIRST) | (u == 2 * FIRST))
+        def waiting():
+            give_back(*unit_of(u - FIRST // 2 - u // (2 * FIRST)))
+
+        @pl.when(h == 0)
+        def inner():
+            activations(c)
+
+        for half, first in ((0, 0), (1, FIRST)):
+
+            @pl.when(u == first)
+            def down_weights(half=half):
+                swaps[4 + half].wait_recv()
+
+        outputs(c, h)
+
+        @pl.when((u >= FIRST) & (u < 2 * FIRST))
+        def next_rows():
+            arrive(u)
+
+        @pl.when(u == 2 * FIRST - 1)
+        def one_more():
+            arrive(u + 1)
+
+        @pl.when((u >= 2 * FIRST) & (h == 0) & (c < GROUPS - 3))
+        def later_rows():
+            arrive(c + 3)
+
+        @pl.when((u == 1) | (u == 2 * FIRST))
+        def soon():
+            give_back(*unit_of(u - 1))
+
+        @pl.when(u >= 2 * FIRST + 3)
+        def later():
+            give_back(*unit_of(u - 3))
 
         return 0
 
-    lax.fori_loop(BANDS - 2, BANDS - 1, gather_band, 0)
-    lax.fori_loop(0, N_SP, sent, 0)
+    lax.fori_loop(0, 2 * GROUPS, stage, 0)
+    give_back(GROUPS - 2, 1)
+    lax.fori_loop(0, 1, gather_band, 0)
+    give_back(GROUPS - 1, 0)
+    give_back(GROUPS - 1, 1)
+    lax.fori_loop(1, BANDS - 1, gather_band, 0)
     for c in range(GROUPS):
         cross(c, recv, xrecv, x_send, x_recv).wait_send()
         for half in range(2):
             cross_back(c, half).wait_send()
     for copy in [halo_copy, *swaps, *stat_copies, *far_copies, *near_copies[0], *near_copies[1]]:
         copy.wait_send()
-    gather_band(BANDS - 1, 0)
+
+    def sent(k, _):
+        @pl.when(k != SELF)
+        def away():
+            wait_for(recv.at[k], d_send.at[k])
+            for h in range(2):
+                wait_for(fin.at[k, :, pl.ds(0, half_width)], r_send.at[2 * k + h])
+
+        return 0
+
+    lax.fori_loop(0, N_SP, sent, 0)
+    lax.fori_loop(BANDS - 1, BANDS, gather_band, 0)
 
     def last_norm(i, _):
         at = pl.ds(pl.multiple_of(i * strip, strip), strip)
@@ -578,16 +624,17 @@
             moved,
             moved,
             pltpu.VMEM((2 * count, width), BF16),
-            pltpu.VMEM((2 * count, 2 * units), BF16),
-            pltpu.VMEM((2, count, width), F32),
+            pltpu.VMEM((GROUPS, 2 * count, 2 * units), BF16),
+            pltpu.VMEM((GROUPS, count, width), F32),
             moved,
             moved,
             moved,
             dma((experts,)), dma((experts,)),
             dma((GROUPS,)), dma((GROUPS,)),
             dma((2 * GROUPS,)), dma((2 * GROUPS,)),
-            dma((experts,)), dma((experts,)),
-            dma((5,)), dma((5,)), dma((13,)),
+            dma((2 * experts,)), dma((2 * experts,)),
+            dma((6,)), dma((6,)), dma((13,)),
+            pltpu.SemaphoreType.REGULAR((6,)),
             dma((2,)), dma((3,)), dma((3,)),
             dma((2,)), dma((2,)), dma((4,)), dma((4,)),
         ],

time: 169 us -> 162 us (0.959)
  Pallas kernels: 167 us -> 160 us
    pallas_call x1, Pallas kernels: 167 us -> 160 us  [shards(): pl.pallas_call(layer_kernel, out_shape=jax.ShapeDtypeStruct((BLOCK, width...]
where the time goes in v5:
time: 162 us
  Pallas kernels  160 us (99%)
  local copies, waits for them, and re-layouts  1.88 us (1%)
    pallas_call x1, Pallas kernels, shards(): pl.pallas_call(layer_kernel, out_shape=jax.ShapeDtypeStruct((BLOCK, width...  160 us

profile of v5, /device:TPU:1, one launch (start us, length us, event | category | flops | bytes accessed | tf_op | source)
XLA Modules:
  0.0 162.1 jit_solution(4599706764848784864)
XLA Ops:
  0.0 160.2 %layer.1 = bf16[128,2048]{1,0:T(8,128)(2,1)} custom-call(bf16[512,512]{1,0:T(8,128)(2,1)} %value_h.1, bf16[512,512]{1,0:T(8,128)(2,1)} %gate_h.1, f32[31,512]{1,0:T(8,128)} %taps_h.1, f32[1,512]{1,0:T(1,128)} %bitcast.7, bf16[128,2048]{1,0:T(8,128)(2,1)} %residual_h.1, f32[1,2048]{1,0:T(1,128)} %bitcast.5, f32[1,2048]{1,0:T(1,128)} %bitcast.6, ...), custom_call_target="tpu_custom_call" | custom-call | tf_op jit(solution)/shard_map/layer/pallas_call | solution.py:585
  160.2 1.9 %copy.15 = bf16[128,2048]{1,0:T(8,128)(2,1)} copy(bf16[128,2048]{1,0:T(8,128)(2,1)} %layer.1) | data formatting | bytes 1048576

commit v6 on v5

--- a/solution.py
+++ b/solution.py
@@ -62,7 +62,7 @@
 def layer_kernel(
     value_h, gate_h, taps_h, norm_gain_h, residual_h, resid_gain_h, out_gain_h, ids_h, weights_h, mix_weight, w_gate, w_up, w_down,
     out,
-    value, gate, taps, norm_gain, residual, resid_gain, out_gain, ids, weights, total_v, ext, halo_send, halo_recv, conv_v, stat_cols, stat_rows, stats_send, stats_recv, mix_in, mix_v,
+    value, gate, taps, norm_gain, residual, resid_gain, out_gain, ids, weights, total_v, out_v, ext, halo_send, halo_recv, conv_v, stat_cols, stat_rows, stats_send, stats_recv, mix_in, mix_v,
     a_send_v, a_recv_v, b_send_v, b_recv_v, acc, hidden, held, share, slots, ret,
     gate_v, up_v, down_v, recv, xrecv, rows_v, act_v, kept, xsend, xret, fin,
     d_send, d_recv, x_send, x_recv, b_send, b_recv, r_send, r_recv, w_send, w_recv, l_sem,
@@ -354,7 +354,7 @@
         if group % 2 == 0:
             fill_slots(group // 2)
         if group == SELF_GROUP:
-            pltpu.make_async_copy(slots.at[SELF], recv.at[SELF], d_recv.at[SELF]).start()
+            pltpu.make_async_copy(slots.at[SELF], recv.at[SELF], d_recv.at[SELF_GROUP]).start()
         for half in range(2):
             dz = step_along_z(group // 2, half)
             base = group * PEERS + half * SIDE
@@ -363,7 +363,7 @@
                 other = peer_at(z, y, core, dz, (1 - group % 2) * SIDE + r, 1)
                 pltpu.make_async_remote_copy(
                     src_ref=slots.at[base + r], dst_ref=recv.at[base + r],
-                    send_sem=d_send.at[base + r], recv_sem=d_recv.at[base + r],
+                    send_sem=d_send.at[0], recv_sem=d_recv.at[group],
                     device_id=(other, tp), device_id_type=MESH,
                 ).start()
                 return 0
@@ -373,7 +373,7 @@
     def cross(c, src, dst, send_sem, recv_sem):
         return pltpu.make_async_remote_copy(
             src_ref=src.at[pl.ds(c * PEERS, PEERS)], dst_ref=dst.at[pl.ds(c * PEERS, PEERS)],
-            send_sem=send_sem.at[c], recv_sem=recv_sem.at[c],
+            send_sem=send_sem.at[0], recv_sem=recv_sem.at[c],
             device_id=(sp, row_partner), device_id_type=MESH,
         )
 
@@ -381,18 +381,14 @@
         at, cols = pl.ds(c * PEERS, PEERS), pl.ds(half * half_width, half_width)
         return pltpu.make_async_remote_copy(
             src_ref=xsend.at[at, :, cols], dst_ref=xret.at[at, :, cols],
-            send_sem=b_send.at[2 * c + half], recv_sem=b_recv.at[2 * c + half],
+            send_sem=b_send.at[0], recv_sem=b_recv.at[2 * c + half],
             device_id=(sp, row_partner), device_id_type=MESH,
         )
 
     count = PEERS * CAP
 
     def arrive(group):
-        def one(r, _):
-            wait_for(recv.at[group * PEERS + r], d_recv.at[group * PEERS + r])
-            return 0
-
-        lax.fori_loop(0, PEERS, one, 0)
+        wait_for(recv.at[pl.ds(group * PEERS, PEERS)], d_recv.at[group])
         cross(group, recv, xrecv, x_send, x_recv).start()
 
     def activations(c):
@@ -442,25 +438,25 @@
                 def away():
                     pltpu.make_async_remote_copy(
                         src_ref=fin.at[k, :, cols], dst_ref=ret.at[k, :, cols],
-                        send_sem=r_send.at[2 * k + h], recv_sem=r_recv.at[2 * k + h],
+                        send_sem=r_send.at[0], recv_sem=r_recv.at[2 * c + h],
                         device_id=(other, tp), device_id_type=MESH,
                     ).start()
 
                 @pl.when(k == SELF)
                 def here():
-                    pltpu.make_async_copy(fin.at[k, :, cols], ret.at[k, :, cols], r_recv.at[2 * k + h]).start()
+                    pltpu.make_async_copy(fin.at[k, :, cols], ret.at[k, :, cols], r_recv.at[2 * c + h]).start()
 
                 return 0
 
             lax.fori_loop(0, SIDE, send, 0)
 
     def gather_band(band, _):
-        def one(r, _):
-            k = band * 2 * PEERS + r // 2
-            wait_for(ret.at[k, :, pl.ds(0, half_width)], r_recv.at[2 * k + r % 2])
-            return 0
-
-        lax.fori_loop(0, 4 * PEERS, one, 0)
+        for i in range(2):
+            group = 2 * band + i
+            for h in range(2):
+                rows = ret.at[pl.ds(group * PEERS, PEERS), :, pl.ds(h * half_width, half_width)]
+                wait_for(rows, r_recv.at[2 * group + h])
+
         own = share[:, pl.ds(pl.multiple_of(band * band_slots, band_slots), band_slots)]
 
         def one_tile(n, _):
@@ -487,9 +483,14 @@
     def stage(u, _):
         c, h = unit_of(u)
 
-        @pl.when((u == FIRST) | (u == 2 * FIRST))
+        @pl.when(u == FIRST)
         def waiting():
-            give_back(*unit_of(u - FIRST // 2 - u // (2 * FIRST)))
+            give_back(1, 0)
+
+        @pl.when(u == 2 * FIRST)
+        def both():
+            give_back(0, 1)
+            give_back(1, 1)
 
         @pl.when(h == 0)
         def inner():
@@ -503,21 +504,18 @@
 
         outputs(c, h)
 
-        @pl.when((u >= FIRST) & (u < 2 * FIRST))
+        @pl.when(u == 2 * FIRST - 1)
         def next_rows():
-            arrive(u)
-
-        @pl.when(u == 2 * FIRST - 1)
-        def one_more():
-            arrive(u + 1)
+            for group in range(FIRST, FIRST + 3):
+                arrive(group)
 
         @pl.when((u >= 2 * FIRST) & (h == 0) & (c < GROUPS - 3))
         def later_rows():
             arrive(c + 3)
 
-        @pl.when((u == 1) | (u == 2 * FIRST))
+        @pl.when(u == 1)
         def soon():
-            give_back(*unit_of(u - 1))
+            give_back(0, 0)
 
         @pl.when(u >= 2 * FIRST + 3)
         def later():
@@ -531,31 +529,28 @@
     give_back(GROUPS - 1, 0)
     give_back(GROUPS - 1, 1)
     lax.fori_loop(1, BANDS - 1, gather_band, 0)
-    for c in range(GROUPS):
-        cross(c, recv, xrecv, x_send, x_recv).wait_send()
-        for half in range(2):
-            cross_back(c, half).wait_send()
+    wait_for(recv, x_send.at[0])
+    wait_for(xsend, b_send.at[0])
     for copy in [halo_copy, *swaps, *stat_copies, *far_copies, *near_copies[0], *near_copies[1]]:
         copy.wait_send()
 
-    def sent(k, _):
-        @pl.when(k != SELF)
-        def away():
-            wait_for(recv.at[k], d_send.at[k])
-            for h in range(2):
-                wait_for(fin.at[k, :, pl.ds(0, half_width)], r_send.at[2 * k + h])
-
-        return 0
-
-    lax.fori_loop(0, N_SP, sent, 0)
+    wait_for(recv.at[pl.ds(0, N_SP - 1)], d_send.at[0])
+    wait_for(fin.at[pl.ds(0, N_SP - 1)], r_send.at[0])
     lax.fori_loop(BANDS - 1, BANDS, gather_band, 0)
 
     def last_norm(i, _):
         at = pl.ds(pl.multiple_of(i * strip, strip), strip)
-        out[at] = normalize(total_v[at], out_gain[...]).astype(BF16)
+        out_v[at] = normalize(total_v[at], out_gain[...]).astype(BF16)
         return 0
 
-    lax.fori_loop(0, BLOCK // strip, last_norm, 0, unroll=True)
+    pieces = []
+    for i in range(2):
+        at = pl.ds(i * BLOCK // 2, BLOCK // 2)
+        lax.fori_loop(i * BLOCK // strip // 2, (i + 1) * BLOCK // strip // 2, last_norm, 0, unroll=True)
+        pieces.append(pltpu.make_async_copy(out_v.at[at], out.at[at], l_sem.at[i]))
+        pieces[-1].start()
+    for piece in pieces:
+        piece.wait()
 
 
 def shards(
@@ -586,7 +581,7 @@
         layer_kernel,
         out_shape=jax.ShapeDtypeStruct((BLOCK, width), BF16),
         in_specs=[hbm] * 13,
-        out_specs=vmem,
+        out_specs=hbm,
         scratch_shapes=[
             pltpu.VMEM(glu_value.shape, BF16),
             pltpu.VMEM(glu_gate.shape, BF16),
@@ -598,6 +593,7 @@
             pltpu.VMEM((2, BLOCK), jnp.int32),
             pltpu.VMEM((2, BLOCK), F32),
             pltpu.VMEM((BLOCK, width), F32),
+            pltpu.VMEM((BLOCK, width), BF16),
             pltpu.VMEM((groups, ROWS + HALO, LANES), F32),
             pltpu.VMEM((groups, HALO, LANES), BF16),
             pltpu.VMEM((groups, HALO, LANES), BF16),
@@ -629,10 +625,10 @@
             moved,
             moved,
             moved,
-            dma((experts,)), dma((experts,)),
-            dma((GROUPS,)), dma((GROUPS,)),
-            dma((2 * GROUPS,)), dma((2 * GROUPS,)),
-            dma((2 * experts,)), dma((2 * experts,)),
+            dma((1,)), dma((GROUPS,)),
+            dma((1,)), dma((GROUPS,)),
+            dma((1,)), dma((2 * GROUPS,)),
+            dma((1,)), dma((2 * GROUPS,)),
             dma((6,)), dma((6,)), dma((13,)),
             pltpu.SemaphoreType.REGULAR((6,)),
             dma((2,)), dma((3,)), dma((3,)),

time: 162 us -> 159 us (0.981)
  Pallas kernels: 160 us -> 157 us
    pallas_call x1, Pallas kernels: 160 us -> 157 us  [shards(): pl.pallas_call(layer_kernel, out_shape=jax.ShapeDtypeStruct((BLOCK, width...]
where the time goes in v6:
time: 159 us
  Pallas kernels  157 us (99%)
  local copies, waits for them, and re-layouts  1.88 us (1%)
    pallas_call x1, Pallas kernels, shards(): pl.pallas_call(layer_kernel, out_shape=jax.ShapeDtypeStruct((BLOCK, width...  157 us

profile of v6, /device:TPU:1, one launch (start us, length us, event | category | flops | bytes accessed | tf_op | source)
XLA Modules:
  0.0 159.0 jit_solution(6115101390168090068)
XLA Ops:
  0.0 157.1 %layer.1 = bf16[128,2048]{1,0:T(8,128)(2,1)} custom-call(bf16[512,512]{1,0:T(8,128)(2,1)} %value_h.1, bf16[512,512]{1,0:T(8,128)(2,1)} %gate_h.1, f32[31,512]{1,0:T(8,128)} %taps_h.1, f32[1,512]{1,0:T(1,128)} %bitcast.7, bf16[128,2048]{1,0:T(8,128)(2,1)} %residual_h.1, f32[1,2048]{1,0:T(1,128)} %bitcast.5, f32[1,2048]{1,0:T(1,128)} %bitcast.6, ...), custom_call_target="tpu_custom_call" | custom-call | tf_op jit(solution)/shard_map/layer/pallas_call | solution.py:580
  157.1 1.9 %copy.15 = bf16[128,2048]{1,0:T(8,128)(2,1)} copy(bf16[128,2048]{1,0:T(8,128)(2,1)} %layer.1) | data formatting | bytes 1048576
